TPU v7x, 512 devices: a 8x2x16 block of a 8x16x16 slice. The times are simulated.
512 devices in a mesh: grp: 2 (over y), tp: 16 (over z), dp: 16 (over x, core).
Axes of the slice: x: 8, y: 2, z: 16, core: 2. Of those that a mesh axis runs over, the one named last changes fastest.
The devices are a block of a 8x16x16 slice.
Arguments:
- tokens: bfloat16 [1024, 4096], P(('grp', 'tp'), 'dp'), parts along dimension 0, may hold values from -6 to 6
- lengths: int32 [256], P(('grp', 'dp')), parts along dimension 0, may hold values from 1 to 4, as said below
- norm_gain: float32 [2, 4096], P(None, 'dp'), may hold values from 0.1 to 1.9
- w_recept: bfloat16 [2, 4096, 2048], P(None, 'dp', 'tp'), may hold values from -0.09375 to 0.09375
- w_keys: bfloat16 [2, 4096, 2048], P(None, 'dp', 'tp'), may hold values from -0.09375 to 0.09375
- w_values: bfloat16 [2, 4096, 2048], P(None, 'dp', 'tp'), may hold values from -0.09375 to 0.09375
- w_decay: bfloat16 [2, 4096, 2048], P(None, 'dp', 'tp'), may hold values from -0.09375 to 0.09375
- w_rate: bfloat16 [2, 4096, 2048], P(None, 'dp', 'tp'), may hold values from -0.09375 to 0.09375
- w_gate: bfloat16 [2, 4096, 2048], P(None, 'dp', 'tp'), may hold values from -0.09375 to 0.09375
- decay_base: float32 [2, 2048], P(None, 'tp'), may hold values from -3 to 1
- group_gain: float32 [2, 2048], P(None, 'tp'), may hold values from 0.1 to 1.9
- w_out: bfloat16 [2, 2048, 4096], P(None, 'tp', 'dp'), may hold values from -0.125 to 0.125
- states: float32 [2, 256, 32, 4096], P(None, ('grp', 'dp'), 'tp'), parts along dimension 1, may hold values from -2 to 2
Outputs:
- tokens_out: bfloat16 [1024, 4096], P(('grp', 'tp'), 'dp'), parts along dimension 0
- states_out: float32 [2, 256, 32, 4096], P(None, ('grp', 'dp'), 'tp'), parts along dimension 1
There are 2 independent parts, one for each index of `grp`. A program takes and returns all parts, laid end to end along the dimension named above; an argument that names none is the same for every part. Nothing has to cross between parts.
Inputs may be any that keep to these rules, and one draw needn't show every extreme that they name: Sequence s has its first lengths[s] of its 4 slots live; in every draw all 8 sequences of some index of dp have 4 live slots.
All inputs are finite; a program needn't handle non-finite values.
Results may differ from a plain program's by a relative error of at most 0.029.
Values may be sent and summed in bfloat16 or wider, within the bound.
A program may use at most 64 MiB of HBM per device.

v0:
```python
import jax
import jax.numpy as jnp
from jax import lax
from jax.sharding import PartitionSpec as P

D = 4096
HEAD = 64
NEW = 4


norm_epsilon = 1e-06
unit_epsilon = 0.00064
group_epsilon = 0.00064


def laid_out(blocks, dim):
    blocks = jnp.moveaxis(blocks, 0, dim)
    dims = blocks.shape
    return blocks.reshape(*dims[:dim], dims[dim] * dims[dim + 1], *dims[dim + 2 :])


def copy_for_each(x, axis):
    copies = jnp.broadcast_to(x, (lax.axis_size(axis), *x.shape))
    return lax.all_to_all(copies, axis, split_axis=0, concat_axis=0, tiled=True)


def gather_directly(x, axis, dim):
    return laid_out(copy_for_each(x, axis), dim)


def of_everyone(x, axis):
    return copy_for_each(x, axis).sum(axis=0)


def cut_along(x, dim, size):
    dims = x.shape
    blocks = x.reshape(*dims[:dim], size, dims[dim] // size, *dims[dim + 1 :])
    return jnp.moveaxis(blocks, dim, 0)


def summed_on_arrival(x, axis, dim):
    blocks = cut_along(x, dim, lax.axis_size(axis))
    arrived = lax.all_to_all(blocks, axis, split_axis=0, concat_axis=0, tiled=True)
    return arrived.sum(axis=0)


def sent_and_summed(x, axis, dim):
    size = lax.axis_size(axis)
    blocks = lax.all_to_all(cut_along(x, dim, size), axis, 0, 0, tiled=True)
    return jnp.sum(blocks.astype(jnp.float32), axis=0)


def advance(state_in, pieces, lengths, base_log, gain_vec):
    seq_count = state_in.shape[0]
    head_count = state_in.shape[1]
    head_shape = (seq_count, NEW, head_count, HEAD)
    recept, keys, values, decay_pre, rate_pre, gate_pre = [
        piece.astype(jnp.float32).reshape(head_shape) for piece in pieces
    ]
    decays = jnp.exp(
        -jnp.exp(-jax.nn.softplus(-(base_log.reshape(head_count, HEAD) + decay_pre)) - 0.5)
    )
    rates = jax.nn.sigmoid(rate_pre)
    unit_keys = keys * lax.rsqrt(jnp.sum(keys * keys, -1, keepdims=True) + unit_epsilon)
    memory = state_in.reshape(seq_count, head_count, HEAD, HEAD)
    live_mask = jnp.arange(NEW)[None, :] < lengths[:, None]
    readings = []
    for position in range(NEW):
        unit_now = unit_keys[:, position]
        removed = jnp.einsum("shvk,shk->shv", memory, unit_now)
        updated = (
            memory * decays[:, position][:, :, None, :]
            - removed[..., None] * (unit_now * rates[:, position])[:, :, None, :]
            + values[:, position][..., None] * keys[:, position][:, :, None, :]
        )
        live_now = live_mask[:, position][:, None, None, None]
        memory = jnp.where(live_now, updated, memory)
        readings.append(jnp.einsum("shvk,shk->shv", memory, recept[:, position]))
    outputs_h = jnp.stack(readings, 1)
    head_mean = jnp.mean(outputs_h, -1, keepdims=True)
    head_var = jnp.mean(jnp.square(outputs_h - head_mean), -1, keepdims=True)
    normed = (
        (outputs_h - head_mean)
        * lax.rsqrt(head_var + group_epsilon)
        * gain_vec.reshape(head_count, HEAD)
    )
    mixed_out = normed * jax.nn.sigmoid(gate_pre) * live_mask[:, :, None, None].astype(jnp.float32)
    return (
        memory.reshape(state_in.shape),
        mixed_out.reshape(seq_count * NEW, head_count * HEAD).astype(jnp.bfloat16),
    )


def per_device(
    tokens,
    lengths,
    norm_gain,
    w_recept,
    w_keys,
    w_values,
    w_decay,
    w_rate,
    w_gate,
    decay_base,
    group_gain,
    w_out,
    states,
):
    gathered = gather_directly(tokens, "tp", 0)
    own_count = gathered.shape[0] // lax.axis_size("dp")
    row_start = lax.axis_index("dp") * own_count
    width_dev = w_recept.shape[2]
    own_rows = tokens
    new_states = []
    for layer_id in range(2):
        wide_rows = gathered.astype(jnp.float32)
        square = of_everyone(jnp.sum(wide_rows * wide_rows, -1), "dp")
        inv_rms = lax.rsqrt(
            lax.dynamic_slice_in_dim(square, row_start, own_count, 0) / D + norm_epsilon
        )[:, None]
        scaled = (wide_rows * norm_gain[layer_id]).astype(jnp.bfloat16)
        matrices = [
            matrix[layer_id] for matrix in (w_recept, w_keys, w_values, w_decay, w_rate, w_gate)
        ]

        def project():
            return jnp.concatenate(
                [
                    jnp.dot(scaled, matrix, preferred_element_type=jnp.float32)
                    for matrix in matrices
                ],
                1,
            )

        summed = summed_on_arrival(project(), "dp", 0)
        pieces = [
            (inv_rms * summed[:, role_id * width_dev : (role_id + 1) * width_dev]).astype(
                jnp.bfloat16
            )
            for role_id in range(6)
        ]
        memory, mixed_out = advance(
            states[layer_id], pieces, lengths, decay_base[layer_id], group_gain[layer_id]
        )
        new_states.append(memory)
        out_weight = w_out[layer_id]
        partial_value = jnp.dot(
            gather_directly(mixed_out, "dp", 0), out_weight, preferred_element_type=jnp.float32
        )
        shared_sum = sent_and_summed(partial_value.astype(jnp.bfloat16), "tp", 0)
        own_rows = (own_rows.astype(jnp.float32) + shared_sum).astype(jnp.bfloat16)
        if layer_id == 0:
            gathered = gather_directly(own_rows, "tp", 0)
    return (own_rows, jnp.stack(new_states))


def solution(mesh):
    placed = (
        P(("grp", "tp"), "dp"),
        P(("grp", "dp")),
        P(None, "dp"),
        P(None, "dp", "tp"),
        P(None, "dp", "tp"),
        P(None, "dp", "tp"),
        P(None, "dp", "tp"),
        P(None, "dp", "tp"),
        P(None, "dp", "tp"),
        P(None, "tp"),
        P(None, "tp"),
        P(None, "tp", "dp"),
        P(None, ("grp", "dp"), "tp", None),
    )
    return jax.shard_map(
        per_device,
        mesh=mesh,
        in_specs=placed,
        out_specs=(P(("grp", "tp"), "dp"), P(None, ("grp", "dp"), "tp", None)),
        check_vma=False,
    )
```

profile of v0, /device:TPU:81, one launch (start us, length us, event | category | flops | bytes accessed | tf_op | source)
XLA Modules:
  0.0 303.8 jit_solution(11342835664175332296)
XLA Ops:
  0.7 1.5 broadcast_in_dim.105
  2.2 43.4 %all-to-all-start = ((bf16[16,32,256]{2,1,0:T(8,128)(2,1)}), bf16[16,32,256]{2,1,0:T(8,128)(2,1)S(1)}, u32[]{:S(2)}, u32[]{:S(2)}) async-start(bf16[16,32,256]{2,1,0:T(8,128)(2,1)} %broadcast_in_dim.105), calls=%async_computation | async-start | bytes 524288 | tf_op jit(solution)/shard_map/all_to_all | solution.py:24
  46.9 12.3 %all-to-all-done = bf16[16,32,256]{2,1,0:T(8,128)(2,1)S(1)} async-done(((bf16[16,32,256]{2,1,0:T(8,128)(2,1)}), bf16[16,32,256]{2,1,0:T(8,128)(2,1)S(1)}, u32[]{:S(2)}, u32[]{:S(2)}) %all-to-all-start) | async-done | bytes 262176 | tf_op jit(solution)/shard_map/all_to_all | solution.py:24
  60.0 12.8 %all-to-all-start.1 = ((f32[16,1,512]{2,1,0:T(1,128)}), f32[16,1,512]{2,1,0:T(1,128)S(1)}, u32[]{:S(2)}, u32[]{:S(2)}) async-start(f32[16,1,512]{2,1,0:T(1,128)} %broadcast_in_dim.107), calls=%async_computation.1 | async-start | bytes 65536 | tf_op jit(solution)/shard_map/all_to_all | solution.py:24
  75.1 1.6 copy.40
  76.7 3.5 %all-to-all-done.1 = f32[16,1,512]{2,1,0:T(1,128)S(1)} async-done(((f32[16,1,512]{2,1,0:T(1,128)}), f32[16,1,512]{2,1,0:T(1,128)S(1)}, u32[]{:S(2)}, u32[]{:S(2)}) %all-to-all-start.1) | async-done | bytes 32800 | tf_op jit(solution)/shard_map/all_to_all | solution.py:24
  80.8 3.9 %all-to-all-start.2 = ((f32[16,32,768]{2,1,0:T(8,128)}), f32[16,32,768]{2,1,0:T(8,128)S(1)}, u32[]{:S(2)}, u32[]{:S(2)}) async-start(f32[16,32,768]{2,1,0:T(8,128)} %bitcast.8), calls=%async_computation.2 | async-start | bytes 3145728 | tf_op jit(solution)/shard_map/all_to_all | solution.py:43
  87.6 35.8 %all-to-all-done.2 = f32[16,32,768]{2,1,0:T(8,128)S(1)} async-done(((f32[16,32,768]{2,1,0:T(8,128)}), f32[16,32,768]{2,1,0:T(8,128)S(1)}, u32[]{:S(2)}, u32[]{:S(2)}) %all-to-all-start.2) | async-done | bytes 1572896 | tf_op jit(solution)/shard_map/all_to_all | solution.py:43
  127.5 1.4 broadcast_multiply_fusion.11
  130.6 13.0 %all_to_all.52 = bf16[16,32,128]{2,1,0:T(8,128)(2,1)S(1)} all-to-all(bf16[16,32,128]{2,1,0:T(8,128)(2,1)S(1)} %broadcast_in_dim.114), channel_id=1, replica_groups=mesh['grp'=2,'tp'=16,'dp'=16] {'dp'}, dimensions={0} | all-to-all | bytes 262144 | tf_op jit(solution)/shard_map/all_to_all | solution.py:24
  143.8 19.9 %all_to_all.53 = bf16[16,32,256]{2,1,0:T(8,128)(2,1)S(1)} all-to-all(bf16[16,32,256]{2,1,0:T(8,128)(2,1)S(1)} %bitcast.352), channel_id=1, replica_groups=mesh['grp'=2,'tp'=16,'dp'=16] {'tp'}, dimensions={0} | all-to-all | bytes 524288 | tf_op jit(solution)/shard_map/all_to_all | solution.py:49
  163.8 23.7 %all_to_all.54 = bf16[16,32,256]{2,1,0:T(8,128)(2,1)S(1)} all-to-all(bf16[16,32,256]{2,1,0:T(8,128)(2,1)S(1)} %broadcast_in_dim.115), channel_id=1, replica_groups=mesh['grp'=2,'tp'=16,'dp'=16] {'tp'}, dimensions={0} | all-to-all | bytes 524288 | tf_op jit(solution)/shard_map/all_to_all | solution.py:24
  188.3 9.2 %all-to-all-start.6 = ((f32[16,1,512]{2,1,0:T(1,128)}), f32[16,1,512]{2,1,0:T(1,128)}, u32[]{:S(2)}, u32[]{:S(2)}) async-start(f32[16,1,512]{2,1,0:T(1,128)} %broadcast_in_dim.117), calls=%async_computation.6 | async-start | bytes 65536 | tf_op jit(solution)/shard_map/all_to_all | solution.py:24
  199.8 1.6 copy.46
  201.4 3.8 %all-to-all-done.6 = f32[16,1,512]{2,1,0:T(1,128)} async-done(((f32[16,1,512]{2,1,0:T(1,128)}), f32[16,1,512]{2,1,0:T(1,128)}, u32[]{:S(2)}, u32[]{:S(2)}) %all-to-all-start.6) | async-done | bytes 32800 | tf_op jit(solution)/shard_map/all_to_all | solution.py:24
  205.3 4.2 %all-to-all-start.7 = ((f32[16,32,768]{2,1,0:T(8,128)}), f32[16,32,768]{2,1,0:T(8,128)S(1)}, u32[]{:S(2)}, u32[]{:S(2)}) async-start(f32[16,32,768]{2,1,0:T(8,128)} %bitcast.77), calls=%async_computation.7 | async-start | bytes 3145728 | tf_op jit(solution)/shard_map/all_to_all | solution.py:43
  214.0 2.1 mul.944
  218.0 2.1 mul.935
  223.5 3.7 %add_select_fusion.7 = (f32[1,8,2,4096]{3,2,1,0:T(2,128)}, f32[1,8,2,4096]{3,2,1,0:T(2,128)S(1)}) fusion(f32[1,8,2,4096]{3,2,1,0:T(2,128)} %mul.944, f32[1,8,2,4096]{3,2,1,0:T(2,128)S(1)} %mul.943, f32[1,8,2,4096]{3,2,1,0:T(2,128)S(1)} %mul.941, f32[1,8,2,4096]{3,2,1,0:T(2,128)} %mul.940, f32[1,8,2,4096]{3,2,1,0:T(2,128)} %mul.939, ...), kind=kLoop, calls=%fused_computation.42 | loop fusion | flops 1048576 | bytes 4194336 | tf_op jit(solution)/shard_map/jit(_where)/select_n | solution.py:77
  228.4 19.6 %all-to-all-done.7 = f32[16,32,768]{2,1,0:T(8,128)S(1)} async-done(((f32[16,32,768]{2,1,0:T(8,128)}), f32[16,32,768]{2,1,0:T(8,128)S(1)}, u32[]{:S(2)}, u32[]{:S(2)}) %all-to-all-start.7) | async-done | bytes 1572896 | tf_op jit(solution)/shard_map/all_to_all | solution.py:43
  253.9 4.2 %all-to-all-start.8 = ((bf16[16,32,128]{2,1,0:T(8,128)(2,1)}), bf16[16,32,128]{2,1,0:T(8,128)(2,1)S(1)}, u32[]{:S(2)}, u32[]{:S(2)}) async-start(bf16[16,32,128]{2,1,0:T(8,128)(2,1)} %broadcast_in_dim.118), calls=%async_computation.8 | async-start | bytes 262144 | tf_op jit(solution)/shard_map/all_to_all | solution.py:24
  261.2 1.5 mul.897
  262.8 2.0 mul.953
  264.8 1.5 mul.885
  266.3 2.0 mul.949
  268.3 1.5 mul.866
  269.9 2.0 mul.945
  271.9 2.0 mul.960
  281.7 1.8 convolution_convert_fusion
  283.4 5.9 %all-to-all-start.9 = ((bf16[16,32,256]{2,1,0:T(8,128)(2,1)}), bf16[16,32,256]{2,1,0:T(8,128)(2,1)S(1)}, u32[]{:S(2)}, u32[]{:S(2)}) async-start(bf16[16,32,256]{2,1,0:T(8,128)(2,1)} %bitcast.137), calls=%async_computation.9 | async-start | bytes 524288 | tf_op jit(solution)/shard_map/all_to_all | solution.py:49
  289.4 2.4 add_select_fusion.6
  292.9 10.3 %all-to-all-done.9 = bf16[16,32,256]{2,1,0:T(8,128)(2,1)S(1)} async-done(((bf16[16,32,256]{2,1,0:T(8,128)(2,1)}), bf16[16,32,256]{2,1,0:T(8,128)(2,1)S(1)}, u32[]{:S(2)}, u32[]{:S(2)}) %all-to-all-start.9) | async-done | bytes 262176 | tf_op jit(solution)/shard_map/all_to_all | solution.py:49
  (271 shorter events, 46.1 us)
Async XLA Ops:
  0.6 73.2 %copy-start.15 = (bf16[2,256,128]{2,1,0:T(8,128)(2,1)S(1)}, bf16[2,256,128]{2,1,0:T(8,128)(2,1)}, u32[]{:S(2)}) copy-start(bf16[2,256,128]{2,1,0:T(8,128)(2,1)} %param.17) | copy-start | bytes 393220
  0.6 73.5 %copy-start.16 = (bf16[2,256,128]{2,1,0:T(8,128)(2,1)S(1)}, bf16[2,256,128]{2,1,0:T(8,128)(2,1)}, u32[]{:S(2)}) copy-start(bf16[2,256,128]{2,1,0:T(8,128)(2,1)} %param.18) | copy-start | bytes 393220
  0.7 73.7 %copy-start.18 = (bf16[2,256,128]{2,1,0:T(8,128)(2,1)S(1)}, bf16[2,256,128]{2,1,0:T(8,128)(2,1)}, u32[]{:S(2)}) copy-start(bf16[2,256,128]{2,1,0:T(8,128)(2,1)} %param.19) | copy-start | bytes 393220
  2.2 57.0 %all-to-all-start = ((bf16[16,32,256]{2,1,0:T(8,128)(2,1)}), bf16[16,32,256]{2,1,0:T(8,128)(2,1)S(1)}, u32[]{:S(2)}, u32[]{:S(2)}) async-start(bf16[16,32,256]{2,1,0:T(8,128)(2,1)} %broadcast_in_dim.105), calls=%async_computation | async-start | bytes 524288 | tf_op jit(solution)/shard_map/all_to_all | solution.py:24
  45.6 29.0 %copy-start.20 = (bf16[2,256,128]{2,1,0:T(8,128)(2,1)S(1)}, bf16[2,256,128]{2,1,0:T(8,128)(2,1)}, u32[]{:S(2)}) copy-start(bf16[2,256,128]{2,1,0:T(8,128)(2,1)} %param.20) | copy-start | bytes 393220
  59.3 15.5 %copy-start.22 = (bf16[2,256,128]{2,1,0:T(8,128)(2,1)S(1)}, bf16[2,256,128]{2,1,0:T(8,128)(2,1)}, u32[]{:S(2)}) copy-start(bf16[2,256,128]{2,1,0:T(8,128)(2,1)} %param.21) | copy-start | bytes 393220
  60.0 20.2 %all-to-all-start.1 = ((f32[16,1,512]{2,1,0:T(1,128)}), f32[16,1,512]{2,1,0:T(1,128)S(1)}, u32[]{:S(2)}, u32[]{:S(2)}) async-start(f32[16,1,512]{2,1,0:T(1,128)} %broadcast_in_dim.107), calls=%async_computation.1 | async-start | bytes 65536 | tf_op jit(solution)/shard_map/all_to_all | solution.py:24
  80.8 42.6 %all-to-all-start.2 = ((f32[16,32,768]{2,1,0:T(8,128)}), f32[16,32,768]{2,1,0:T(8,128)S(1)}, u32[]{:S(2)}, u32[]{:S(2)}) async-start(f32[16,32,768]{2,1,0:T(8,128)} %bitcast.8), calls=%async_computation.2 | async-start | bytes 3145728 | tf_op jit(solution)/shard_map/all_to_all | solution.py:43
  85.5 45.0 %copy-start.53 = (f32[32]{0:T(128)}, f32[32]{0:T(128)S(1)}, u32[]{:S(2)}) copy-start(f32[32]{0:T(128)S(1)} %reshape.764) | copy-start | bytes 388
  86.1 38.7 %copy-start.51 = (pred[8]{0:T(512)(128)(4,1)}, pred[8]{0:T(512)(128)(4,1)S(1)}, u32[]{:S(2)}) copy-start(pred[8]{0:T(512)(128)(4,1)S(1)} %get-tuple-element.7) | copy-start | bytes 28
  86.1 39.6 %copy-start.49 = (pred[8]{0:T(512)(128)(4,1)}, pred[8]{0:T(512)(128)(4,1)S(1)}, u32[]{:S(2)}) copy-start(pred[8]{0:T(512)(128)(4,1)S(1)} %get-tuple-element.6) | copy-start | bytes 28
  86.1 41.4 %copy-start.47 = (pred[8]{0:T(512)(128)(4,1)}, pred[8]{0:T(512)(128)(4,1)S(1)}, u32[]{:S(2)}) copy-start(pred[8]{0:T(512)(128)(4,1)S(1)} %get-tuple-element.5) | copy-start | bytes 28
  86.1 43.2 %copy-start.55 = (pred[8]{0:T(512)(128)(4,1)}, pred[8]{0:T(512)(128)(4,1)S(1)}, u32[]{:S(2)}) copy-start(pred[8]{0:T(512)(128)(4,1)S(1)} %get-tuple-element.4) | copy-start | bytes 28
  87.6 35.9 %copy-start.58 = (f32[32]{0:T(128)}, f32[32]{0:T(128)S(1)}, u32[]{:S(2)}) copy-start(f32[32]{0:T(128)S(1)} %add_rsqrt_fusion.5) | copy-start | bytes 388
  128.9 14.7 %copy-start.23 = (bf16[2,128,256]{2,1,0:T(8,128)(2,1)S(1)}, bf16[2,128,256]{2,1,0:T(8,128)(2,1)}, u32[]{:S(2)}) copy-start(bf16[2,128,256]{2,1,0:T(8,128)(2,1)} %param.24) | copy-start | bytes 393220
  129.4 34.4 %copy-start.34 = (bf16[32,256]{1,0:T(8,128)(2,1)S(1)}, bf16[32,256]{1,0:T(8,128)(2,1)}, u32[]{:S(2)}) copy-start(bf16[32,256]{1,0:T(8,128)(2,1)} %param.13) | copy-start | bytes 49156
  129.9 57.6 %copy-start.57 = (f32[1,256]{1,0:T(1,128)S(1)}, f32[1,256]{1,0:T(1,128)}, u32[]{:S(2)}) copy-start(f32[1,256]{1,0:T(1,128)} %get-tuple-element.94) | copy-start | bytes 3076
  130.6 66.9 %copy-start.14 = (bf16[2,256,128]{2,1,0:T(8,128)(2,1)S(1)}, bf16[2,256,128]{2,1,0:T(8,128)(2,1)}, u32[]{:S(2)}) copy-start(bf16[2,256,128]{2,1,0:T(8,128)(2,1)} %param.16) | copy-start | bytes 393220
  163.7 34.3 %copy-start.17 = (bf16[2,256,128]{2,1,0:T(8,128)(2,1)S(1)}, bf16[2,256,128]{2,1,0:T(8,128)(2,1)}, u32[]{:S(2)}) copy-start(bf16[2,256,128]{2,1,0:T(8,128)(2,1)} %param.18) | copy-start | bytes 393220
  163.8 34.5 %copy-start.19 = (bf16[2,256,128]{2,1,0:T(8,128)(2,1)S(1)}, bf16[2,256,128]{2,1,0:T(8,128)(2,1)}, u32[]{:S(2)}) copy-start(bf16[2,256,128]{2,1,0:T(8,128)(2,1)} %param.19) | copy-start | bytes 393220
  187.5 11.0 %copy-start.21 = (bf16[2,256,128]{2,1,0:T(8,128)(2,1)S(1)}, bf16[2,256,128]{2,1,0:T(8,128)(2,1)}, u32[]{:S(2)}) copy-start(bf16[2,256,128]{2,1,0:T(8,128)(2,1)} %param.20) | copy-start | bytes 393220
  188.3 16.9 %all-to-all-start.6 = ((f32[16,1,512]{2,1,0:T(1,128)}), f32[16,1,512]{2,1,0:T(1,128)}, u32[]{:S(2)}, u32[]{:S(2)}) async-start(f32[16,1,512]{2,1,0:T(1,128)} %broadcast_in_dim.117), calls=%async_computation.6 | async-start | bytes 65536 | tf_op jit(solution)/shard_map/all_to_all | solution.py:24
  205.3 42.7 %all-to-all-start.7 = ((f32[16,32,768]{2,1,0:T(8,128)}), f32[16,32,768]{2,1,0:T(8,128)S(1)}, u32[]{:S(2)}, u32[]{:S(2)}) async-start(f32[16,32,768]{2,1,0:T(8,128)} %bitcast.77), calls=%async_computation.7 | async-start | bytes 3145728 | tf_op jit(solution)/shard_map/all_to_all | solution.py:43
  253.9 27.7 %all-to-all-start.8 = ((bf16[16,32,128]{2,1,0:T(8,128)(2,1)}), bf16[16,32,128]{2,1,0:T(8,128)(2,1)S(1)}, u32[]{:S(2)}, u32[]{:S(2)}) async-start(bf16[16,32,128]{2,1,0:T(8,128)(2,1)} %broadcast_in_dim.118), calls=%async_computation.8 | async-start | bytes 262144 | tf_op jit(solution)/shard_map/all_to_all | solution.py:24
  278.7 10.6 %copy-start.4 = (f32[2,8,2,4096]{3,2,1,0:T(2,128)S(1)}, f32[2,8,2,4096]{3,2,1,0:T(2,128)}, u32[]{:S(2)}) copy-start(f32[2,8,2,4096]{3,2,1,0:T(2,128)} %param.25) | copy-start | bytes 1572868
  278.7 10.6 %copy-start.5 = (f32[1,8,2,4096]{3,2,1,0:T(2,128)S(1)}, f32[1,8,2,4096]{3,2,1,0:T(2,128)}, u32[]{:S(2)}) copy-start(f32[1,8,2,4096]{3,2,1,0:T(2,128)} %mul.953) | copy-start | bytes 786436
  278.7 10.6 %copy-start.6 = (f32[1,8,2,4096]{3,2,1,0:T(2,128)S(1)}, f32[1,8,2,4096]{3,2,1,0:T(2,128)}, u32[]{:S(2)}) copy-start(f32[1,8,2,4096]{3,2,1,0:T(2,128)} %mul.949) | copy-start | bytes 786436
  278.7 10.6 %copy-start.7 = (f32[1,8,2,4096]{3,2,1,0:T(2,128)S(1)}, f32[1,8,2,4096]{3,2,1,0:T(2,128)}, u32[]{:S(2)}) copy-start(f32[1,8,2,4096]{3,2,1,0:T(2,128)} %mul.945) | copy-start | bytes 786436
  278.7 10.6 %copy-start.8 = (f32[1,8,2,4096]{3,2,1,0:T(2,128)S(1)}, f32[1,8,2,4096]{3,2,1,0:T(2,128)}, u32[]{:S(2)}) copy-start(f32[1,8,2,4096]{3,2,1,0:T(2,128)} %mul.960) | copy-start | bytes 786436
  278.7 10.6 %copy-start.9 = (f32[1,8,2,4096]{3,2,1,0:T(2,128)S(1)}, f32[1,8,2,4096]{3,2,1,0:T(2,128)}, u32[]{:S(2)}) copy-start(f32[1,8,2,4096]{3,2,1,0:T(2,128)} %mul.947) | copy-start | bytes 786436
  278.7 10.6 %copy-start.10 = (f32[1,8,2,4096]{3,2,1,0:T(2,128)S(1)}, f32[1,8,2,4096]{3,2,1,0:T(2,128)}, u32[]{:S(2)}) copy-start(f32[1,8,2,4096]{3,2,1,0:T(2,128)} %mul.948) | copy-start | bytes 786436
  283.4 19.8 %all-to-all-start.9 = ((bf16[16,32,256]{2,1,0:T(8,128)(2,1)}), bf16[16,32,256]{2,1,0:T(8,128)(2,1)S(1)}, u32[]{:S(2)}, u32[]{:S(2)}) async-start(bf16[16,32,256]{2,1,0:T(8,128)(2,1)} %bitcast.137), calls=%async_computation.9 | async-start | bytes 524288 | tf_op jit(solution)/shard_map/all_to_all | solution.py:49
  (42 other events, 143.6 us)
where the time goes:
time: 310 us; the launch traced here: 304 us
  waiting for transfers between devices  85.2 us (27%)
  starting transfers between devices  83.5 us (27%)
  blocking collectives  56.5 us (18%)
  local copies, waits for them, and re-layouts  46.6 us (15%)
  other arithmetic  19.7 us (6%)
  matrix products  10.6 us (3%)
    all_to_all x4, starting transfers between devices, copy_for_each(): return lax.all_to_all(copies, axis, split_axis=0, concat_axis=0, tiled=True)  69.5 us
    all_to_all x2, waiting for transfers between devices, summed_on_arrival(): lax.all_to_all(blocks, axis, split_axis=0, concat_axis=0, tiled=True)  55.3 us
    all_to_all x2, blocking collectives, copy_for_each(): return lax.all_to_all(copies, axis, split_axis=0, concat_axis=0, tiled=True)  36.6 us
    all_to_all x1, blocking collectives, sent_and_summed(): blocks = lax.all_to_all(cut_along(x, dim, size), axis, 0, 0, tiled=True)  19.9 us
    all_to_all x4, waiting for transfers between devices, copy_for_each(): return lax.all_to_all(copies, axis, split_axis=0, concat_axis=0, tiled=True)  19.6 us
    mul x18, local copies, waits for them, and re-layouts, advance(): memory * decays[:, position][:, :, None, :]  16.1 us
    all_to_all x1, waiting for transfers between devices, sent_and_summed(): blocks = lax.all_to_all(cut_along(x, dim, size), axis, 0, 0, tiled=True)  10.3 us
    mul x11, local copies, waits for them, and re-layouts, advance(): values[:, position][..., None] * keys[:, position][:, :, None, :]  9.89 us
  transfers between devices with their start and end apart: 7, of which 6 were waited for; matrix products, arithmetic and copies ran while one was open for 19% of the time, Pallas kernels for 0%

commit v1 on v0

v1 whole, which is shorter than its diff:
```python
import functools

import jax
import jax.numpy as jnp
from jax import lax
from jax.experimental import pallas as pl
from jax.experimental.pallas import tpu as pltpu
from jax.sharding import PartitionSpec as P

HEAD = 64
NEW = 4
LANES = 128
norm_epsilon = 1e-06
unit_epsilon = 0.00064
group_epsilon = 0.00064
MESH = pl.DeviceIdType.MESH
F32 = jnp.float32
BF16 = jnp.bfloat16


def iota(shape, dim):
    return lax.broadcasted_iota(jnp.int32, shape, dim)


def dot(a, b):
    return jnp.dot(a, b, preferred_element_type=F32)


def dot_split(a, b):
    high = a.astype(BF16)
    low = (a - high.astype(F32)).astype(BF16)
    return dot(high, b) + dot(low, b)


def pair_rows(value):
    high = value.astype(BF16).astype(F32)
    return jnp.concatenate([high, value - high], axis=-2)


def by_distance(n, act):
    act(n // 2)

    def body(step, carry):
        dist = n // 2 - 1 - step
        act(dist)
        act(n - dist)
        return carry

    lax.fori_loop(0, n // 2 - 1, body, 0)


def kernel(
    n_tp, n_dp,
    tokens_ref, lengths_ref, gain_ref, base_ref, group_ref,
    w0, w1, w2, w3, w4, w5, wout_hbm, states_hbm,
    tokens_out, states_out,
    w_v, wo_v, st_v, x_buf, pair_out, pair_in, own_part, rs_out, rs_in, mix_buf, part_out, part_in,
    local_sem, st_sem, z_send, z_recv, d_send, d_recv, rs_send, rs_recv, pair_send, pair_recv,
):
    t = lax.axis_index("tp")
    d = lax.axis_index("dp")
    n_x = n_dp // 2
    x = d // 2
    c = d % 2
    rows = tokens_ref.shape[0]
    feats = tokens_ref.shape[1]
    seqs = rows // NEW
    width = LANES
    model = feats * n_dp

    loads = []
    for i, w in enumerate((w0, w1, w2, w3, w4, w5)):
        loads.append(
            pltpu.make_async_copy(w, w_v.at[:, :, pl.ds(i * width, width)], local_sem.at[i])
        )
    loads.append(pltpu.make_async_copy(wout_hbm, wo_v, local_sem.at[6]))
    loads.append(pltpu.make_async_copy(states_hbm, st_v, local_sem.at[7]))
    for load in loads:
        load.start()

    barrier = pltpu.get_barrier_semaphore()

    def greet_z(off):
        pl.semaphore_signal(barrier, inc=1, device_id={"tp": lax.rem(t + off, n_tp)}, device_id_type=MESH)

    def greet_d(off):
        pl.semaphore_signal(barrier, inc=1, device_id={"dp": lax.rem(d + off, n_dp)}, device_id_type=MESH)

    by_distance(n_tp, greet_z)
    by_distance(n_dp, greet_d)
    pl.semaphore_wait(barrier, n_tp + n_dp - 2)

    def z_copy(src, dst_of, phase, peer, slot):
        return pltpu.make_async_remote_copy(
            src_ref=src, dst_ref=dst_of(slot),
            send_sem=z_send.at[phase, peer], recv_sem=z_recv.at[phase, slot],
            device_id={"tp": peer}, device_id_type=MESH,
        )

    def d_copy(layer, peer, slot):
        return pltpu.make_async_remote_copy(
            src_ref=mix_buf.at[layer, d], dst_ref=mix_buf.at[layer, slot],
            send_sem=d_send.at[layer, peer], recv_sem=d_recv.at[layer, slot],
            device_id={"dp": peer}, device_id_type=MESH,
        )

    def rs_copy(layer, peer, slot):
        return pltpu.make_async_remote_copy(
            src_ref=rs_out.at[layer, peer], dst_ref=rs_in.at[layer, slot],
            send_sem=rs_send.at[layer, peer], recv_sem=rs_recv.at[layer, slot],
            device_id={"dp": peer * 2 + c}, device_id_type=MESH,
        )

    def pair_copy(layer):
        return pltpu.make_async_remote_copy(
            src_ref=pair_out.at[layer], dst_ref=pair_in.at[layer],
            send_sem=pair_send.at[layer], recv_sem=pair_recv.at[layer],
            device_id={"dp": x * 2 + (1 - c)}, device_id_type=MESH,
        )

    def x_slot(layer):
        return lambda slot: x_buf.at[layer, slot // 2, slot % 2]

    def part_slot(layer):
        return lambda slot: part_in.at[layer, slot]

    lane8 = iota((8, LANES), 1)
    m8 = (lane8 // HEAD) == (iota((8, LANES), 0) % 2)
    sq = (LANES, LANES)
    same_half = ((iota(sq, 0) // HEAD) == (iota(sq, 1) // HEAD)).astype(F32).astype(BF16)
    spread = ((iota(sq, 0) % 2) == (iota(sq, 1) // HEAD)).astype(F32).astype(BF16)
    collect = ((iota(sq, 0) // HEAD) == (iota(sq, 1) % 2)).astype(F32).astype(BF16)
    tall = (HEAD, LANES)
    row_of = iota(tall, 0)
    lane_of = iota(tall, 1)
    entry = (((lane_of // HEAD) == (row_of % 2)) & (((lane_of % HEAD) // 2) == (row_of // 2))).astype(F32)
    entry = entry.reshape(1, 8, 8, LANES)
    tok_row = iota((rows, LANES), 0)
    length_rows = jnp.zeros((rows, LANES), jnp.int32)
    for s in range(seqs):
        length_rows = jnp.where((tok_row // NEW) == s, lengths_ref[s], length_rows)
    live = (tok_row % NEW) < length_rows

    def send_tokens(off):
        z_copy(tokens_ref, x_slot(0), 0, lax.rem(t + off, n_tp), t).start()

    by_distance(n_tp, send_tokens)
    x_buf[0, t // 2, t % 2] = tokens_ref[...]
    own_rows = tokens_ref[...].astype(F32)

    def project(layer, half):
        block = x_buf[layer, :, half]
        wide = block.reshape(n_x * rows, feats).astype(F32)
        total = jnp.sum(wide * wide, axis=-1, keepdims=True)
        total = jnp.broadcast_to(total, (n_x * rows, LANES)).reshape(n_x, rows // 8, 8, LANES)
        group = lane8 // 32
        packed = jnp.where(
            group == 0, total[:, 0],
            jnp.where(group == 1, total[:, 1], jnp.where(group == 2, total[:, 2], total[:, 3])),
        )
        scaled = (wide * gain_ref[pl.ds(layer, 1), :]).astype(BF16)
        return scaled, packed

    for layer in range(2):
        def wait_tokens(off):
            src = lax.rem(t + off, n_tp)
            z_copy(tokens_ref, x_slot(layer), 2 * layer, t, src).wait_recv()

        by_distance(n_tp, wait_tokens)
        if layer == 0:
            for load in loads:
                load.wait()

        scaled, packed = project(layer, 1 - c)
        for j in range(3):
            out = dot(scaled, w_v[layer, :, 2 * width * j : 2 * width * (j + 1)])
            for k in range(2):
                i = 2 * j + k
                piece = out[:, k * width : (k + 1) * width].astype(BF16)
                pair_out[layer, :, i * rows : (i + 1) * rows, :] = piece.reshape(n_x, rows, width)
        pair_out[layer, :, 6 * rows : 6 * rows + 16, :] = pair_rows(packed).astype(BF16)
        pair_copy(layer).start()

        scaled, packed = project(layer, c)
        for j in range(3):
            out = dot(scaled, w_v[layer, :, 2 * width * j : 2 * width * (j + 1)])
            for k in range(2):
                i = 2 * j + k
                own_part[:, i * rows : (i + 1) * rows, :] = out[:, k * width : (k + 1) * width].reshape(n_x, rows, width)
        own_part[:, 6 * rows : 6 * rows + 8, :] = packed
        pair_copy(layer).wait_recv()

        def both(place):
            arrived = pair_in[layer, place].astype(F32)
            main = own_part[place, : 6 * rows] + arrived[: 6 * rows]
            squares = own_part[place, 6 * rows : 6 * rows + 8] + (
                arrived[6 * rows : 6 * rows + 8] + arrived[6 * rows + 8 :]
            )
            return main, squares

        def send_sums(off):
            place = lax.rem(x + off, n_x)
            main, squares = both(place)
            rs_out[layer, place, : 6 * rows] = main.astype(BF16)
            rs_out[layer, place, 6 * rows :] = pair_rows(squares).astype(BF16)
            rs_copy(layer, place, x).start()

        by_distance(n_x, send_sums)
        main, squares = both(x)
        own_part[x, : 6 * rows] = main
        own_part[x, 6 * rows : 6 * rows + 8] = squares

        def add_sums(off):
            src = lax.rem(x + off, n_x)
            rs_copy(layer, x, src).wait_recv()
            arrived = rs_in[layer, src].astype(F32)
            own_part[x, : 6 * rows] += arrived[: 6 * rows]
            own_part[x, 6 * rows : 6 * rows + 8] += arrived[6 * rows : 6 * rows + 8] + arrived[6 * rows + 8 :]

        by_distance(n_x, add_sums)

        squares = own_part[x, 6 * rows : 6 * rows + 8]
        inv = lax.rsqrt(squares / model + norm_epsilon)
        inv_rows = jnp.concatenate(
            [jnp.broadcast_to(inv[:, 32 * g : 32 * g + 1], (8, LANES)) for g in range(rows // 8)], 0
        )
        recept, keys, values, decay_pre, rate_pre, gate_pre = [
            (inv_rows * own_part[x, i * rows : (i + 1) * rows]).astype(BF16).astype(F32) for i in range(6)
        ]
        raw = base_ref[pl.ds(layer, 1), :] + decay_pre
        decays = jnp.exp(-jnp.exp(jnp.float32(-0.5)) / (1.0 + jnp.exp(-raw)))
        rates = 1.0 / (1.0 + jnp.exp(-rate_pre))
        unit = keys * lax.rsqrt(dot_split(keys * keys, same_half) + unit_epsilon)
        zero = jnp.zeros_like(keys)
        decays = jnp.where(live, decays, 1.0)
        drop = jnp.where(live, unit * rates, zero)
        put = jnp.where(live, keys, zero)

        def tile_maker(q):
            turned = pltpu.roll(q, HEAD, 1)

            def tiles(n):
                made = []
                for s in range(seqs):
                    at = NEW * s + n
                    made.append(
                        jnp.where(
                            m8,
                            jnp.broadcast_to(q[at : at + 1], (8, LANES)),
                            jnp.broadcast_to(turned[at : at + 1], (8, LANES)),
                        )
                    )
                return jnp.stack(made)[:, None]

            return tiles

        decay_tiles, unit_tiles, drop_tiles, put_tiles, recept_tiles = [
            tile_maker(q) for q in (decays, unit, drop, put, recept)
        ]
        full = (seqs, 8, 8, LANES)
        flat = (seqs * HEAD, LANES)
        memory = st_v[layer].reshape(full)
        reads = jnp.zeros((rows, LANES), F32)
        for n in range(NEW):
            value_rows = jnp.stack(
                [jnp.broadcast_to(values[NEW * s + n : NEW * s + n + 1], (8, LANES)) for s in range(seqs)]
            )[:, None]
            value_full = dot((value_rows * entry).reshape(flat).astype(BF16), spread).reshape(full)
            removed = dot_split((memory * unit_tiles(n)).reshape(flat), same_half).reshape(full)
            memory = memory * decay_tiles(n) - removed * drop_tiles(n) + value_full * put_tiles(n)
            seen = dot_split((memory * recept_tiles(n)).reshape(flat), collect).reshape(full)
            seen = jnp.sum(seen * entry, axis=1).reshape(seqs * 8, LANES)
            pick_shape = (rows, seqs * 8)
            pick = (iota(pick_shape, 0) == (iota(pick_shape, 1) // 8) * NEW + n).astype(F32).astype(BF16)
            seen_high = seen.astype(BF16)
            seen_low = (seen - seen_high.astype(F32)).astype(BF16)
            reads = reads + dot(pick, seen_high) + dot(pick, seen_low)
        st_v[layer] = memory.reshape(flat)
        pltpu.make_async_copy(st_v.at[layer], states_out.at[layer], st_sem.at[layer]).start()

        mean = dot_split(reads, same_half) / HEAD
        dev = reads - mean
        var = dot_split(dev * dev, same_half) / HEAD
        normed = dev * lax.rsqrt(var + group_epsilon) * group_ref[pl.ds(layer, 1), :]
        mixed = jnp.where(live, normed / (1.0 + jnp.exp(-gate_pre)), zero)
        mix_buf[layer, d] = mixed.astype(BF16)

        def send_mixed(off):
            d_copy(layer, lax.rem(d + off, n_dp), d).start()

        def wait_mixed(off):
            d_copy(layer, d, lax.rem(d + off, n_dp)).wait_recv()

        by_distance(n_dp, send_mixed)
        by_distance(n_dp, wait_mixed)
        partial = dot(mix_buf[layer].reshape(n_dp * rows, width), wo_v[layer])
        part_out[layer] = partial.astype(BF16).reshape(n_tp, rows, feats)

        def send_part(off):
            peer = lax.rem(t + off, n_tp)
            z_copy(part_out.at[layer, peer], part_slot(layer), 2 * layer + 1, peer, t).start()

        by_distance(n_tp, send_part)
        part_in[layer, t] = part_out[layer, t]

        def wait_part(off):
            src = lax.rem(t + off, n_tp)
            z_copy(part_out.at[layer, t], part_slot(layer), 2 * layer + 1, t, src).wait_recv()

        by_distance(n_tp, wait_part)
        own_rows = own_rows + jnp.sum(part_in[layer].astype(F32), axis=0)
        own_rows = own_rows.astype(BF16)
        if layer == 0:
            x_buf[1, t // 2, t % 2] = own_rows

            def send_rows(off):
                z_copy(x_buf.at[1, t // 2, t % 2], x_slot(1), 2, lax.rem(t + off, n_tp), t).start()

            by_distance(n_tp, send_rows)
            own_rows = own_rows.astype(F32)
        else:
            tokens_out[...] = own_rows

    for layer in range(2):
        def drain_z(off):
            peer = lax.rem(t + off, n_tp)
            z_copy(tokens_ref, x_slot(layer), 2 * layer, peer, t).wait_send()
            z_copy(part_out.at[layer, peer], part_slot(layer), 2 * layer + 1, peer, t).wait_send()

        def drain_d(off):
            d_copy(layer, lax.rem(d + off, n_dp), d).wait_send()

        def drain_rs(off):
            rs_copy(layer, lax.rem(x + off, n_x), x).wait_send()

        by_distance(n_tp, drain_z)
        by_distance(n_dp, drain_d)
        by_distance(n_x, drain_rs)
        pair_copy(layer).wait_send()
        pltpu.make_async_copy(st_v.at[layer], states_out.at[layer], st_sem.at[layer]).wait()


def per_device(n_tp, n_dp, tokens, lengths, norm_gain, w_recept, w_keys, w_values, w_decay, w_rate, w_gate,
               decay_base, group_gain, w_out, states):
    rows, feats = tokens.shape
    layers, seqs, heads, flat = states.shape
    folded = flat // LANES
    width = w_recept.shape[2]
    n_x = n_dp // 2
    state_rows = seqs * folded * heads
    packed = states.reshape(layers, seqs, heads, folded, LANES).transpose(0, 1, 3, 2, 4)
    packed = packed.reshape(layers, state_rows, LANES)
    vmem = pl.BlockSpec(memory_space=pltpu.VMEM)
    hbm = pl.BlockSpec(memory_space=pltpu.HBM)
    msg = 6 * rows + 16
    out, new_states = pl.pallas_call(
        functools.partial(kernel, n_tp, n_dp),
        out_shape=(
            jax.ShapeDtypeStruct((rows, feats), BF16),
            jax.ShapeDtypeStruct((layers, state_rows, LANES), F32),
        ),
        in_specs=[vmem, pl.BlockSpec(memory_space=pltpu.SMEM), vmem, vmem, vmem] + [hbm] * 8,
        out_specs=(vmem, hbm),
        scratch_shapes=[
            pltpu.VMEM((layers, feats, 6 * width), BF16),
            pltpu.VMEM((layers, width, feats), BF16),
            pltpu.VMEM((layers, state_rows, LANES), F32),
            pltpu.VMEM((layers, n_tp // 2, 2, rows, feats), BF16),
            pltpu.VMEM((layers, n_x, msg, width), BF16),
            pltpu.VMEM((layers, n_x, msg, width), BF16),
            pltpu.VMEM((n_x, msg, width), F32),
            pltpu.VMEM((layers, n_x, msg, width), BF16),
            pltpu.VMEM((layers, n_x, msg, width), BF16),
            pltpu.VMEM((layers, n_dp, rows, width), BF16),
            pltpu.VMEM((layers, n_tp, rows, feats), BF16),
            pltpu.VMEM((layers, n_tp, rows, feats), BF16),
            pltpu.SemaphoreType.DMA((8,)),
            pltpu.SemaphoreType.DMA((2,)),
            pltpu.SemaphoreType.DMA((4, n_tp)),
            pltpu.SemaphoreType.DMA((4, n_tp)),
            pltpu.SemaphoreType.DMA((2, n_dp)),
            pltpu.SemaphoreType.DMA((2, n_dp)),
            pltpu.SemaphoreType.DMA((2, n_x)),
            pltpu.SemaphoreType.DMA((2, n_x)),
            pltpu.SemaphoreType.DMA((2,)),
            pltpu.SemaphoreType.DMA((2,)),
        ],
        compiler_params=pltpu.CompilerParams(
            collective_id=0, has_side_effects=True, vmem_limit_bytes=48 * 1024 * 1024
        ),
    )(tokens, lengths, norm_gain, decay_base, group_gain,
      w_recept, w_keys, w_values, w_decay, w_rate, w_gate, w_out, packed)
    new_states = new_states.reshape(layers, seqs, folded, heads, LANES).transpose(0, 1, 3, 2, 4)
    return out, new_states.reshape(layers, seqs, heads, flat)


def solution(mesh):
    placed = (
        P(("grp", "tp"), "dp"),
        P(("grp", "dp")),
        P(None, "dp"),
        P(None, "dp", "tp"),
        P(None, "dp", "tp"),
        P(None, "dp", "tp"),
        P(None, "dp", "tp"),
        P(None, "dp", "tp"),
        P(None, "dp", "tp"),
        P(None, "tp"),
        P(None, "tp"),
        P(None, "tp", "dp"),
        P(None, ("grp", "dp"), "tp", None),
    )
    return jax.shard_map(
        functools.partial(per_device, mesh.shape["tp"], mesh.shape["dp"]),
        mesh=mesh,
        in_specs=placed,
        out_specs=(P(("grp", "tp"), "dp"), P(None, ("grp", "dp"), "tp", None)),
        check_vma=False,
    )
```

time: 310 us -> 163 us (0.53); the launches traced: 304 us -> 162 us
  Pallas kernels: 0 us -> 150 us
  waiting for transfers between devices: 85.2 us -> 0 us
  starting transfers between devices: 83.5 us -> 0 us
  blocking collectives: 56.5 us -> 0 us
  local copies, waits for them, and re-layouts: 46.6 us -> 11.5 us
  other arithmetic: 19.7 us -> 0 us
  matrix products: 10.6 us -> 0 us
    pallas_call x0 -> x1, Pallas kernels: none -> 150 us  [per_device(): pl.pallas_call(functools.partial(kernel, n_tp, n_dp), out_shape=(jax.Shap...]
    all_to_all x7 -> x0, waiting for transfers between devices: 85.2 us -> none  [the longest x2 55.3 us: summed_on_arrival(): lax.all_to_all(blocks, axis, split_axis=0, concat_axis=0, tiled=True)]
    all_to_all x7 -> x0, starting transfers between devices: 83.5 us -> none  [the longest x4 69.5 us: copy_for_each(): return lax.all_to_all(copies, axis, split_axis=0, concat_axis=0, tiled=True)]
    all_to_all x3 -> x0, blocking collectives: 56.5 us -> none  [the longest x2 36.6 us: copy_for_each(): return lax.all_to_all(copies, axis, split_axis=0, concat_axis=0, tiled=True)]
    mul x40 -> x0, local copies, waits for them, and re-layouts: 34.9 us -> none  [the longest x18 16.1 us: advance(): memory * decays[:, position][:, :, None, :]]
    unnamed x132 -> x28, local copies, waits for them, and re-layouts: 0.89 us -> 11.5 us
    dot_general x30 -> x0, matrix products: 10.6 us -> none  [the longest x12 4.35 us: project(): jnp.dot(scaled, matrix, preferred_element_type=jnp.float32)]
    mul x16 -> x0, other arithmetic: 7.96 us -> none  [the longest x8 5.48 us: advance(): removed[..., None] * (unit_now * rates[:, position])[:, :, None, :]]
  transfers between devices with their start and end apart: 7 -> 0, of which waited for: 6 -> 0; matrix products, arithmetic and copies ran while one was open for 19% -> 0% of each run, Pallas kernels for 0% -> 0%
where the time goes in v1:
time: 163 us; the launch traced here: 162 us
  Pallas kernels  150 us (92%)
  local copies, waits for them, and re-layouts  11.5 us (7%)
    pallas_call x1, Pallas kernels, per_device(): pl.pallas_call(functools.partial(kernel, n_tp, n_dp), out_shape=(jax.Shap...  150 us
    unnamed x28, local copies, waits for them, and re-layouts  11.5 us

profile of v1, /device:TPU:81, one launch (start us, length us, event | category | flops | bytes accessed | tf_op | source)
XLA Modules:
  0.0 162.2 jit_solution(10798284701573529430)
XLA Ops:
  0.6 0.0 copy-start.10
  0.6 0.0 copy-start.12
  0.7 0.7 copy-done.10
  1.3 0.0 copy-done.12
  1.3 0.0 copy-start
  1.3 1.0 copy-done
  2.4 0.0 copy-start.1
  2.4 0.9 copy-done.1
  3.3 0.0 copy-start.2
  3.3 0.9 copy-done.2
  4.2 0.0 copy-start.3
  4.2 0.9 copy-done.3
  5.1 0.0 copy-start.4
  5.1 0.9 copy-done.4
  6.0 0.0 copy-start.5
  6.0 0.9 copy-done.5
  6.9 0.0 copy-start.6
  6.9 0.9 copy-done.6
  7.8 0.0 copy-start.7
  7.8 0.9 copy-done.7
  8.7 0.0 copy-start.8
  8.7 0.7 copy-done.8
  9.4 0.0 copy-start.9
  9.4 0.7 copy-done.9
  10.1 0.0 copy-start.11
  10.1 0.7 copy-done.11
  10.8 150.0 %shard_map.140 = (bf16[32,256]{1,0:T(8,128)(2,1)S(1)}, f32[2,512,128]{2,1,0:T(8,128)S(1)}) custom-call(bf16[32,256]{1,0:T(8,128)(2,1)S(1)} %copy-done.8, s32[8]{0:T(128)S(1)} %copy-done.12, f32[2,256]{1,0:T(2,128)S(1)} %copy-done.9, f32[2,128]{1,0:T(2,128)S(1)} %copy-done.10, f32[2,128]{1,0:T(2,128)S(1)} %copy-done.11, bf16[2,256,128]{2,1,0:T(8,128)(2,1)S(1)} %copy-done.1, ...), custom_call_target="tpu_custom_call" | custom-call | tf_op jit(solution)/shard_map/pallas_call | solution.py:356
  160.8 0.6 copy.19
  161.4 0.8 copy.20
Async XLA Ops:
  0.6 0.7 copy-start.10
  0.6 0.7 copy-start.12
  1.3 1.0 copy-start
  2.4 0.9 copy-start.1
  3.3 0.9 copy-start.2
  4.2 0.9 copy-start.3
  5.1 0.9 copy-start.4
  6.0 0.9 copy-start.5
  6.9 0.9 copy-start.6
  7.8 0.9 copy-start.7
  8.7 0.7 copy-start.8
  9.4 0.7 copy-start.9
  10.1 0.7 copy-start.11

commit v2 on v1

--- a/solution.py
+++ b/solution.py
@@ -51,24 +51,35 @@
 
 def kernel(
     n_tp, n_dp,
-    tokens_ref, lengths_ref, gain_ref, base_ref, group_ref,
+    tokens_hbm, lengths_hbm, gain_hbm, base_hbm, group_hbm,
     w0, w1, w2, w3, w4, w5, wout_hbm, states_hbm,
     tokens_out, states_out,
-    w_v, wo_v, st_v, x_buf, pair_out, pair_in, own_part, rs_out, rs_in, mix_buf, part_out, part_in,
-    local_sem, st_sem, z_send, z_recv, d_send, d_recv, rs_send, rs_recv, pair_send, pair_recv,
+    tokens_ref, lengths_ref, gain_ref, base_ref, group_ref,
+    w_v, wo_v, st_v, x_buf, pair_out, pair_in, own_part, rs_out, rs_in, mix_buf,
+    part_out, part_in, class_sum, far_out, far_in,
+    local_sem, st_sem, g_send, g_recv, p_send, p_recv, d_send, d_recv, rs_send, rs_recv, pair_send, pair_recv,
 ):
     t = lax.axis_index("tp")
     d = lax.axis_index("dp")
     n_x = n_dp // 2
     x = d // 2
     c = d % 2
-    rows = tokens_ref.shape[0]
-    feats = tokens_ref.shape[1]
+    rows, feats = tokens_ref.shape
     seqs = rows // NEW
     width = LANES
     model = feats * n_dp
-
-    loads = []
+    hops = n_tp // 4
+    near_first = sorted(range(hops), key=lambda j: min(j, hops - j))
+    far_first = near_first[::-1]
+
+    first = pltpu.make_async_copy(tokens_hbm, tokens_ref, local_sem.at[8])
+    first.start()
+    loads = [
+        pltpu.make_async_copy(gain_hbm, gain_ref, local_sem.at[9]),
+        pltpu.make_async_copy(base_hbm, base_ref, local_sem.at[10]),
+        pltpu.make_async_copy(group_hbm, group_ref, local_sem.at[11]),
+        pltpu.make_async_copy(lengths_hbm, lengths_ref, local_sem.at[12]),
+    ]
     for i, w in enumerate((w0, w1, w2, w3, w4, w5)):
         loads.append(
             pltpu.make_async_copy(w, w_v.at[:, :, pl.ds(i * width, width)], local_sem.at[i])
@@ -78,22 +89,48 @@
     for load in loads:
         load.start()
 
+    def around(off):
+        return lax.rem(t + off + 2 * n_tp, n_tp)
+
+    skip = 2 - 4 * (t % 2)
+    targets = (1, -1, skip)
+    sources = (-1, 1, -skip)
+
     barrier = pltpu.get_barrier_semaphore()
 
     def greet_z(off):
-        pl.semaphore_signal(barrier, inc=1, device_id={"tp": lax.rem(t + off, n_tp)}, device_id_type=MESH)
+        pl.semaphore_signal(barrier, inc=1, device_id={"tp": around(off)}, device_id_type=MESH)
 
     def greet_d(off):
         pl.semaphore_signal(barrier, inc=1, device_id={"dp": lax.rem(d + off, n_dp)}, device_id_type=MESH)
 
-    by_distance(n_tp, greet_z)
+    for j in far_first:
+        if j:
+            greet_z(4 * j)
+    for off in targets + sources[2:]:
+        greet_z(off)
     by_distance(n_dp, greet_d)
-    pl.semaphore_wait(barrier, n_tp + n_dp - 2)
-
-    def z_copy(src, dst_of, phase, peer, slot):
-        return pltpu.make_async_remote_copy(
-            src_ref=src, dst_ref=dst_of(slot),
-            send_sem=z_send.at[phase, peer], recv_sem=z_recv.at[phase, slot],
+    first.wait()
+    pl.semaphore_wait(barrier, (hops - 1) + 4 + n_dp - 1)
+
+    def g_copy(layer, src, block, peer, k):
+        return pltpu.make_async_remote_copy(
+            src_ref=src, dst_ref=x_buf.at[layer, block],
+            send_sem=g_send.at[layer, k], recv_sem=g_recv.at[layer, block],
+            device_id={"tp": peer}, device_id_type=MESH,
+        )
+
+    def near_copy(layer, j, i, block, peer):
+        return pltpu.make_async_remote_copy(
+            src_ref=part_out.at[layer, block], dst_ref=part_in.at[layer, 3 * j + i],
+            send_sem=p_send.at[layer, 3 * j + i], recv_sem=p_recv.at[layer, 3 * j + i],
+            device_id={"tp": peer}, device_id_type=MESH,
+        )
+
+    def far_copy(layer, j, peer):
+        return pltpu.make_async_remote_copy(
+            src_ref=far_out.at[layer, j], dst_ref=far_in.at[layer, j],
+            send_sem=p_send.at[layer, 3 * hops + j - 1], recv_sem=p_recv.at[layer, 3 * hops + j - 1],
             device_id={"tp": peer}, device_id_type=MESH,
         )
 
@@ -111,18 +148,36 @@
             device_id={"dp": peer * 2 + c}, device_id_type=MESH,
         )
 
-    def pair_copy(layer):
-        return pltpu.make_async_remote_copy(
-            src_ref=pair_out.at[layer], dst_ref=pair_in.at[layer],
-            send_sem=pair_send.at[layer], recv_sem=pair_recv.at[layer],
+    def pair_copy(layer, place):
+        return pltpu.make_async_remote_copy(
+            src_ref=pair_out.at[layer, place], dst_ref=pair_in.at[layer, place],
+            send_sem=pair_send.at[layer, place], recv_sem=pair_recv.at[layer, place],
             device_id={"dp": x * 2 + (1 - c)}, device_id_type=MESH,
         )
 
-    def x_slot(layer):
-        return lambda slot: x_buf.at[layer, slot // 2, slot % 2]
-
-    def part_slot(layer):
-        return lambda slot: part_in.at[layer, slot]
+    def gather_start(layer, src):
+        for j in far_first:
+            if j:
+                g_copy(layer, src, t, around(4 * j), 3 * hops + j - 1).start()
+        for i, off in enumerate(targets):
+            g_copy(layer, src, t, around(off), i).start()
+
+    def gather_forward(layer, j):
+        block = around(4 * j)
+        g_copy(layer, x_buf.at[layer, block], block, t, 0).wait_recv()
+        for i, off in enumerate(targets):
+            g_copy(layer, x_buf.at[layer, block], block, around(off), 3 * j + i).start()
+
+    def gather_near(layer, j):
+        for off in sources:
+            block = around(off + 4 * j)
+            g_copy(layer, x_buf.at[layer, block], block, t, 0).wait_recv()
+
+    gather_start(0, tokens_ref)
+    x_buf[0, t] = tokens_ref[...]
+    own_rows = tokens_ref[...].astype(F32)
+    for load in loads:
+        load.wait()
 
     lane8 = iota((8, LANES), 1)
     m8 = (lane8 // HEAD) == (iota((8, LANES), 0) % 2)
@@ -141,74 +196,78 @@
         length_rows = jnp.where((tok_row // NEW) == s, lengths_ref[s], length_rows)
     live = (tok_row % NEW) < length_rows
 
-    def send_tokens(off):
-        z_copy(tokens_ref, x_slot(0), 0, lax.rem(t + off, n_tp), t).start()
-
-    by_distance(n_tp, send_tokens)
-    x_buf[0, t // 2, t % 2] = tokens_ref[...]
-    own_rows = tokens_ref[...].astype(F32)
-
-    def project(layer, half):
-        block = x_buf[layer, :, half]
-        wide = block.reshape(n_x * rows, feats).astype(F32)
+    odd = (t + c) % 2
+    even = 1 - odd
+    mine = (-odd, odd - even * skip)
+    theirs = (-even, even - odd * skip)
+
+    def wave(layer, j):
+        blocks = [around(off + 4 * j) for off in theirs + mine]
+        wide = jnp.concatenate([x_buf[layer, block] for block in blocks], 0).astype(F32)
         total = jnp.sum(wide * wide, axis=-1, keepdims=True)
-        total = jnp.broadcast_to(total, (n_x * rows, LANES)).reshape(n_x, rows // 8, 8, LANES)
+        total = jnp.broadcast_to(total, (4 * rows, LANES)).reshape(4, rows // 8, 8, LANES)
         group = lane8 // 32
         packed = jnp.where(
             group == 0, total[:, 0],
             jnp.where(group == 1, total[:, 1], jnp.where(group == 2, total[:, 2], total[:, 3])),
         )
         scaled = (wide * gain_ref[pl.ds(layer, 1), :]).astype(BF16)
-        return scaled, packed
+        for p in range(3):
+            out = dot(scaled, w_v[layer, :, 2 * width * p : 2 * width * (p + 1)])
+            for k in range(2):
+                i = 2 * p + k
+                piece = out[:, k * width : (k + 1) * width].reshape(4, rows, width)
+                for q in range(2):
+                    pair_out[layer, blocks[q] // 2, i * rows : (i + 1) * rows] = piece[q].astype(BF16)
+                    own_part[blocks[2 + q] // 2, i * rows : (i + 1) * rows] = piece[2 + q]
+        for q in range(2):
+            pair_out[layer, blocks[q] // 2, 6 * rows :] = pair_rows(packed[q]).astype(BF16)
+            own_part[blocks[2 + q] // 2, 6 * rows : 6 * rows + 8] = packed[2 + q]
+        for q in range(2):
+            pair_copy(layer, blocks[q] // 2).start()
+
+    def both(layer, place):
+        arrived = pair_in[layer, place].astype(F32)
+        main = own_part[place, : 6 * rows] + arrived[: 6 * rows]
+        squares = own_part[place, 6 * rows : 6 * rows + 8] + (
+            arrived[6 * rows : 6 * rows + 8] + arrived[6 * rows + 8 :]
+        )
+        return main, squares
+
+    def finish(layer, j):
+        for off in mine:
+            place = around(off + 4 * j) // 2
+            pair_copy(layer, place).wait_recv()
+            main, squares = both(layer, place)
+
+            @pl.when(place != x)
+            def _():
+                rs_out[layer, place, : 6 * rows] = main.astype(BF16)
+                rs_out[layer, place, 6 * rows :] = pair_rows(squares).astype(BF16)
+                rs_copy(layer, place, x).start()
+
+            @pl.when(place == x)
+            def _():
+                own_part[x, : 6 * rows] = main
+                own_part[x, 6 * rows : 6 * rows + 8] = squares
 
     for layer in range(2):
-        def wait_tokens(off):
-            src = lax.rem(t + off, n_tp)
-            z_copy(tokens_ref, x_slot(layer), 2 * layer, t, src).wait_recv()
-
-        by_distance(n_tp, wait_tokens)
-        if layer == 0:
-            for load in loads:
-                load.wait()
-
-        scaled, packed = project(layer, 1 - c)
-        for j in range(3):
-            out = dot(scaled, w_v[layer, :, 2 * width * j : 2 * width * (j + 1)])
-            for k in range(2):
-                i = 2 * j + k
-                piece = out[:, k * width : (k + 1) * width].astype(BF16)
-                pair_out[layer, :, i * rows : (i + 1) * rows, :] = piece.reshape(n_x, rows, width)
-        pair_out[layer, :, 6 * rows : 6 * rows + 16, :] = pair_rows(packed).astype(BF16)
-        pair_copy(layer).start()
-
-        scaled, packed = project(layer, c)
-        for j in range(3):
-            out = dot(scaled, w_v[layer, :, 2 * width * j : 2 * width * (j + 1)])
-            for k in range(2):
-                i = 2 * j + k
-                own_part[:, i * rows : (i + 1) * rows, :] = out[:, k * width : (k + 1) * width].reshape(n_x, rows, width)
-        own_part[:, 6 * rows : 6 * rows + 8, :] = packed
-        pair_copy(layer).wait_recv()
-
-        def both(place):
-            arrived = pair_in[layer, place].astype(F32)
-            main = own_part[place, : 6 * rows] + arrived[: 6 * rows]
-            squares = own_part[place, 6 * rows : 6 * rows + 8] + (
-                arrived[6 * rows : 6 * rows + 8] + arrived[6 * rows + 8 :]
-            )
-            return main, squares
-
-        def send_sums(off):
-            place = lax.rem(x + off, n_x)
-            main, squares = both(place)
-            rs_out[layer, place, : 6 * rows] = main.astype(BF16)
-            rs_out[layer, place, 6 * rows :] = pair_rows(squares).astype(BF16)
-            rs_copy(layer, place, x).start()
-
-        by_distance(n_x, send_sums)
-        main, squares = both(x)
-        own_part[x, : 6 * rows] = main
-        own_part[x, 6 * rows : 6 * rows + 8] = squares
+        gather_near(layer, 0)
+        wave(layer, 0)
+        for j in near_first[1:-1]:
+            gather_forward(layer, j)
+        finish(layer, 0)
+        for j in near_first[1:][-1:]:
+            gather_forward(layer, j)
+        for j in near_first[1:-1]:
+            gather_near(layer, j)
+            wave(layer, j)
+        for j in near_first[1:-1]:
+            finish(layer, j)
+        for j in near_first[1:][-1:]:
+            gather_near(layer, j)
+            wave(layer, j)
+            finish(layer, j)
 
         def add_sums(off):
             src = lax.rem(x + off, n_x)
@@ -288,55 +347,61 @@
         def send_mixed(off):
             d_copy(layer, lax.rem(d + off, n_dp), d).start()
 
-        def wait_mixed(off):
-            d_copy(layer, d, lax.rem(d + off, n_dp)).wait_recv()
-
         by_distance(n_dp, send_mixed)
-        by_distance(n_dp, wait_mixed)
-        partial = dot(mix_buf[layer].reshape(n_dp * rows, width), wo_v[layer])
-        part_out[layer] = partial.astype(BF16).reshape(n_tp, rows, feats)
-
-        def send_part(off):
-            peer = lax.rem(t + off, n_tp)
-            z_copy(part_out.at[layer, peer], part_slot(layer), 2 * layer + 1, peer, t).start()
-
-        by_distance(n_tp, send_part)
-        part_in[layer, t] = part_out[layer, t]
-
-        def wait_part(off):
-            src = lax.rem(t + off, n_tp)
-            z_copy(part_out.at[layer, t], part_slot(layer), 2 * layer + 1, t, src).wait_recv()
-
-        by_distance(n_tp, wait_part)
-        own_rows = own_rows + jnp.sum(part_in[layer].astype(F32), axis=0)
+        for j in far_first:
+            blocks = [around(off + 4 * j) for off in targets + (0,)]
+            for block in blocks:
+                @pl.when(block != d)
+                def _():
+                    d_copy(layer, d, block).wait_recv()
+
+            partial = dot(jnp.concatenate([mix_buf[layer, block] for block in blocks], 0), wo_v[layer])
+            partial = partial.reshape(4, rows, feats)
+            for i, off in enumerate(targets):
+                part_out[layer, blocks[i]] = partial[i].astype(BF16)
+                near_copy(layer, j, i, blocks[i], around(off)).start()
+            class_sum[j] = partial[3]
+        for j in far_first:
+            total = class_sum[j]
+            for i in range(3):
+                near_copy(layer, j, i, t, t).wait_recv()
+                total = total + part_in[layer, 3 * j + i].astype(F32)
+            if j:
+                far_out[layer, j] = total.astype(BF16)
+                far_copy(layer, j, around(4 * j)).start()
+            else:
+                own_rows = own_rows + total
+        for j in near_first[1:]:
+            far_copy(layer, j, t).wait_recv()
+            own_rows = own_rows + far_in[layer, j].astype(F32)
         own_rows = own_rows.astype(BF16)
         if layer == 0:
-            x_buf[1, t // 2, t % 2] = own_rows
-
-            def send_rows(off):
-                z_copy(x_buf.at[1, t // 2, t % 2], x_slot(1), 2, lax.rem(t + off, n_tp), t).start()
-
-            by_distance(n_tp, send_rows)
+            x_buf[1, t] = own_rows
+            gather_start(1, x_buf.at[1, t])
             own_rows = own_rows.astype(F32)
         else:
             tokens_out[...] = own_rows
 
     for layer in range(2):
-        def drain_z(off):
-            peer = lax.rem(t + off, n_tp)
-            z_copy(tokens_ref, x_slot(layer), 2 * layer, peer, t).wait_send()
-            z_copy(part_out.at[layer, peer], part_slot(layer), 2 * layer + 1, peer, t).wait_send()
+        for k in range(n_tp - 1):
+            g_copy(layer, tokens_ref, t, t, k).wait_send()
+        for j in range(hops):
+            for i in range(3):
+                near_copy(layer, j, i, t, t).wait_send()
+            if j:
+                far_copy(layer, j, t).wait_send()
 
         def drain_d(off):
             d_copy(layer, lax.rem(d + off, n_dp), d).wait_send()
 
         def drain_rs(off):
-            rs_copy(layer, lax.rem(x + off, n_x), x).wait_send()
-
-        by_distance(n_tp, drain_z)
+            place = lax.rem(x + off, n_x)
+            rs_copy(layer, place, x).wait_send()
+            pair_copy(layer, place).wait_send()
+
         by_distance(n_dp, drain_d)
         by_distance(n_x, drain_rs)
-        pair_copy(layer).wait_send()
+        pair_copy(layer, x).wait_send()
         pltpu.make_async_copy(st_v.at[layer], states_out.at[layer], st_sem.at[layer]).wait()
 
 
@@ -359,13 +424,18 @@
             jax.ShapeDtypeStruct((rows, feats), BF16),
             jax.ShapeDtypeStruct((layers, state_rows, LANES), F32),
         ),
-        in_specs=[vmem, pl.BlockSpec(memory_space=pltpu.SMEM), vmem, vmem, vmem] + [hbm] * 8,
+        in_specs=[hbm] * 13,
         out_specs=(vmem, hbm),
         scratch_shapes=[
+            pltpu.VMEM((rows, feats), BF16),
+            pltpu.SMEM((seqs,), jnp.int32),
+            pltpu.VMEM((layers, feats), F32),
+            pltpu.VMEM((layers, width), F32),
+            pltpu.VMEM((layers, width), F32),
             pltpu.VMEM((layers, feats, 6 * width), BF16),
             pltpu.VMEM((layers, width, feats), BF16),
             pltpu.VMEM((layers, state_rows, LANES), F32),
-            pltpu.VMEM((layers, n_tp // 2, 2, rows, feats), BF16),
+            pltpu.VMEM((layers, n_tp, rows, feats), BF16),
             pltpu.VMEM((layers, n_x, msg, width), BF16),
             pltpu.VMEM((layers, n_x, msg, width), BF16),
             pltpu.VMEM((n_x, msg, width), F32),
@@ -373,20 +443,25 @@
             pltpu.VMEM((layers, n_x, msg, width), BF16),
             pltpu.VMEM((layers, n_dp, rows, width), BF16),
             pltpu.VMEM((layers, n_tp, rows, feats), BF16),
-            pltpu.VMEM((layers, n_tp, rows, feats), BF16),
-            pltpu.SemaphoreType.DMA((8,)),
+            pltpu.VMEM((layers, 3 * n_tp // 4, rows, feats), BF16),
+            pltpu.VMEM((n_tp // 4, rows, feats), F32),
+            pltpu.VMEM((layers, n_tp // 4, rows, feats), BF16),
+            pltpu.VMEM((layers, n_tp // 4, rows, feats), BF16),
+            pltpu.SemaphoreType.DMA((13,)),
             pltpu.SemaphoreType.DMA((2,)),
-            pltpu.SemaphoreType.DMA((4, n_tp)),
-            pltpu.SemaphoreType.DMA((4, n_tp)),
+            pltpu.SemaphoreType.DMA((2, n_tp)),
+            pltpu.SemaphoreType.DMA((2, n_tp)),
+            pltpu.SemaphoreType.DMA((2, n_tp)),
+            pltpu.SemaphoreType.DMA((2, n_tp)),
             pltpu.SemaphoreType.DMA((2, n_dp)),
             pltpu.SemaphoreType.DMA((2, n_dp)),
             pltpu.SemaphoreType.DMA((2, n_x)),
             pltpu.SemaphoreType.DMA((2, n_x)),
-            pltpu.SemaphoreType.DMA((2,)),
-            pltpu.SemaphoreType.DMA((2,)),
+            pltpu.SemaphoreType.DMA((2, n_x)),
+            pltpu.SemaphoreType.DMA((2, n_x)),
         ],
         compiler_params=pltpu.CompilerParams(
-            collective_id=0, has_side_effects=True, vmem_limit_bytes=48 * 1024 * 1024
+            collective_id=0, has_side_effects=True, vmem_limit_bytes=67043328
         ),
     )(tokens, lengths, norm_gain, decay_base, group_gain,
       w_recept, w_keys, w_values, w_decay, w_rate, w_gate, w_out, packed)

time: 163 us -> 139 us (0.85)
  Pallas kernels: 150 us -> 133 us
  local copies, waits for them, and re-layouts: 11.5 us -> 3.21 us
    pallas_call x1, Pallas kernels: 150 us -> 133 us  [per_device(): pl.pallas_call(functools.partial(kernel, n_tp, n_dp), out_shape=(jax.Shap...]
    unnamed x28 -> x2, local copies, waits for them, and re-layouts: 11.5 us -> 3.21 us
where the time goes in v2:
time: 139 us; the launch traced here: 137 us
  Pallas kernels  133 us (96%)
  local copies, waits for them, and re-layouts  3.21 us (2%)
    pallas_call x1, Pallas kernels, per_device(): pl.pallas_call(functools.partial(kernel, n_tp, n_dp), out_shape=(jax.Shap...  133 us
    unnamed x2, local copies, waits for them, and re-layouts  3.21 us

profile of v2, /device:TPU:81, one launch (start us, length us, event | category | flops | bytes accessed | tf_op | source)
XLA Modules:
  0.0 137.3 jit_solution(1913867918339647590)
XLA Ops:
  0.6 133.4 %shard_map.140 = (bf16[32,256]{1,0:T(8,128)(2,1)}, f32[2,512,128]{2,1,0:T(8,128)}) custom-call(bf16[32,256]{1,0:T(8,128)(2,1)} %tokens_hbm.1, s32[8]{0:T(128)} %lengths_hbm.1, f32[2,256]{1,0:T(2,128)} %gain_hbm.1, f32[2,128]{1,0:T(2,128)} %base_hbm.1, f32[2,128]{1,0:T(2,128)} %group_hbm.1, bf16[2,256,128]{2,1,0:T(8,128)(2,1)} %w0.1, ...), custom_call_target="tpu_custom_call" | custom-call | tf_op jit(solution)/shard_map/pallas_call | solution.py:421
  134.1 1.3 copy.19
  135.4 1.9 %copy.20 = f32[2,8,2,4096]{3,2,1,0:T(2,128)} copy(f32[2,8,2,4096]{3,2,1,0:T(2,128)} %bitcast.11) | data formatting | bytes 1048576

commit v3 on v2

v3 whole, which is shorter than its diff:
```python
import functools

import jax
import jax.numpy as jnp
from jax import lax
from jax.experimental import pallas as pl
from jax.experimental.pallas import tpu as pltpu
from jax.sharding import PartitionSpec as P

HEAD = 64
NEW = 4
LANES = 128
HALVES = 2
norm_epsilon = 1e-06
unit_epsilon = 0.00064
group_epsilon = 0.00064
MESH = pl.DeviceIdType.MESH
F32 = jnp.float32
BF16 = jnp.bfloat16


def iota(shape, dim):
    return lax.broadcasted_iota(jnp.int32, shape, dim)


def dot(a, b):
    return jnp.dot(a, b, preferred_element_type=F32)


def dot_split(a, b):
    high = a.astype(BF16)
    low = (a - high.astype(F32)).astype(BF16)
    return dot(high, b) + dot(low, b)


def pair_rows(value):
    high = value.astype(BF16).astype(F32)
    return jnp.concatenate([high, value - high], axis=-2)


def by_distance(n, act):
    act(n // 2)

    def body(step, carry):
        dist = n // 2 - 1 - step
        act(dist)
        act(n - dist)
        return carry

    lax.fori_loop(0, n // 2 - 1, body, 0)


def kernel(
    n_tp, n_dp,
    tokens_hbm, lengths_hbm, gain_hbm, base_hbm, group_hbm,
    w0, w1, w2, w3, w4, w5, wout_hbm, states_hbm,
    tokens_out, states_out,
    tokens_ref, lengths_ref, gain_ref, base_ref, group_ref,
    w_v, wo_v, st_v, x_buf, pair_out, pair_in, own_part, rs_out, rs_in, mix_buf,
    part_out, part_in, class_sum, far_out, far_in,
    local_sem, g_send, g_recv, p_send, p_recv, d_send, d_recv, rs_send, rs_recv, pair_send, pair_recv,
):
    t = lax.axis_index("tp")
    d = lax.axis_index("dp")
    n_x = n_dp // 2
    x = d // 2
    c = d % 2
    _, rows, feats = tokens_ref.shape
    seqs = rows // NEW
    width = LANES
    model = feats * n_dp
    hops = n_tp // 4
    near_first = sorted(range(hops), key=lambda j: min(j, hops - j))
    far_first = near_first[::-1]

    first = [
        pltpu.make_async_copy(tokens_hbm.at[pl.ds(h * rows, rows)], tokens_ref.at[h], local_sem.at[8 + 5 * h])
        for h in range(HALVES)
    ]
    for load in first:
        load.start()
    loads = [
        pltpu.make_async_copy(gain_hbm, gain_ref, local_sem.at[9]),
        pltpu.make_async_copy(base_hbm, base_ref, local_sem.at[10]),
        pltpu.make_async_copy(group_hbm, group_ref, local_sem.at[11]),
        pltpu.make_async_copy(lengths_hbm, lengths_ref, local_sem.at[12]),
    ]
    for i, w in enumerate((w0, w1, w2, w3, w4, w5)):
        loads.append(
            pltpu.make_async_copy(w, w_v.at[:, :, pl.ds(i * width, width)], local_sem.at[i])
        )
    loads.append(pltpu.make_async_copy(wout_hbm, wo_v, local_sem.at[6]))
    loads.append(pltpu.make_async_copy(states_hbm, st_v, local_sem.at[7]))
    for load in loads:
        load.start()

    def around(off):
        return lax.rem(t + off + 2 * n_tp, n_tp)

    skip = 2 - 4 * (t % 2)
    targets = (1, -1, skip)
    sources = (-1, 1, -skip)

    barrier = pltpu.get_barrier_semaphore()

    def greet_z(off):
        pl.semaphore_signal(barrier, inc=1, device_id={"tp": around(off)}, device_id_type=MESH)

    def greet_d(off):
        pl.semaphore_signal(barrier, inc=1, device_id={"dp": lax.rem(d + off, n_dp)}, device_id_type=MESH)

    for j in far_first:
        if j:
            greet_z(4 * j)
    for off in targets + sources[2:]:
        greet_z(off)
    by_distance(n_dp, greet_d)
    for load in first:
        load.wait()
    pl.semaphore_wait(barrier, (hops - 1) + 4 + n_dp - 1)

    def g_copy(chain, src, block, peer, k):
        return pltpu.make_async_remote_copy(
            src_ref=src, dst_ref=x_buf.at[chain, block],
            send_sem=g_send.at[chain, k], recv_sem=g_recv.at[chain, block],
            device_id={"tp": peer}, device_id_type=MESH,
        )

    def near_copy(chain, j, i, block, peer):
        return pltpu.make_async_remote_copy(
            src_ref=part_out.at[chain, block], dst_ref=part_in.at[chain, 3 * j + i],
            send_sem=p_send.at[chain, 3 * j + i], recv_sem=p_recv.at[chain, 3 * j + i],
            device_id={"tp": peer}, device_id_type=MESH,
        )

    def far_copy(chain, j, peer):
        return pltpu.make_async_remote_copy(
            src_ref=far_out.at[chain, j], dst_ref=far_in.at[chain, j],
            send_sem=p_send.at[chain, 3 * hops + j - 1], recv_sem=p_recv.at[chain, 3 * hops + j - 1],
            device_id={"tp": peer}, device_id_type=MESH,
        )

    def d_copy(chain, peer, slot):
        return pltpu.make_async_remote_copy(
            src_ref=mix_buf.at[chain, d], dst_ref=mix_buf.at[chain, slot],
            send_sem=d_send.at[chain, peer], recv_sem=d_recv.at[chain, slot],
            device_id={"dp": peer}, device_id_type=MESH,
        )

    def rs_copy(chain, peer, slot):
        return pltpu.make_async_remote_copy(
            src_ref=rs_out.at[chain, peer], dst_ref=rs_in.at[chain, slot],
            send_sem=rs_send.at[chain, peer], recv_sem=rs_recv.at[chain, slot],
            device_id={"dp": peer * 2 + c}, device_id_type=MESH,
        )

    def pair_copy(chain, place):
        return pltpu.make_async_remote_copy(
            src_ref=pair_out.at[chain, place], dst_ref=pair_in.at[chain, place],
            send_sem=pair_send.at[chain, place], recv_sem=pair_recv.at[chain, place],
            device_id={"dp": x * 2 + (1 - c)}, device_id_type=MESH,
        )

    def gather_start(chain, src):
        for j in far_first:
            if j:
                g_copy(chain, src, t, around(4 * j), 3 * hops + j - 1).start()
        for i, off in enumerate(targets):
            g_copy(chain, src, t, around(off), i).start()

    def gather_forward(chain, j):
        block = around(4 * j)
        g_copy(chain, x_buf.at[chain, block], block, t, 0).wait_recv()
        for i, off in enumerate(targets):
            g_copy(chain, x_buf.at[chain, block], block, around(off), 3 * j + i).start()

    def gather_near(chain, j):
        for off in sources:
            block = around(off + 4 * j)
            g_copy(chain, x_buf.at[chain, block], block, t, 0).wait_recv()

    for h in range(HALVES):
        gather_start(h, tokens_ref.at[h])
    for h in range(HALVES):
        x_buf[h, t] = tokens_ref[h]
    own_rows = [tokens_ref[h].astype(F32) for h in range(HALVES)]
    for load in loads:
        load.wait()

    lane8 = iota((8, LANES), 1)
    m8 = (lane8 // HEAD) == (iota((8, LANES), 0) % 2)
    sq = (LANES, LANES)
    same_half = ((iota(sq, 0) // HEAD) == (iota(sq, 1) // HEAD)).astype(F32).astype(BF16)
    spread = ((iota(sq, 0) % 2) == (iota(sq, 1) // HEAD)).astype(F32).astype(BF16)
    collect = ((iota(sq, 0) // HEAD) == (iota(sq, 1) % 2)).astype(F32).astype(BF16)
    tall = (HEAD, LANES)
    row_of = iota(tall, 0)
    lane_of = iota(tall, 1)
    entry = (((lane_of // HEAD) == (row_of % 2)) & (((lane_of % HEAD) // 2) == (row_of // 2))).astype(F32)
    entry = entry.reshape(1, 8, 8, LANES)
    tok_row = iota((rows, LANES), 0)
    live_rows = []
    for h in range(HALVES):
        length_rows = jnp.zeros((rows, LANES), jnp.int32)
        for q in range(seqs):
            length_rows = jnp.where((tok_row // NEW) == q, lengths_ref[h * seqs + q], length_rows)
        live_rows.append((tok_row % NEW) < length_rows)
    groups = rows // 8
    span = LANES // groups

    odd = (t + c) % 2
    even = 1 - odd
    mine = (-odd, odd - even * skip)
    theirs = (-even, even - odd * skip)

    def wave(layer, h, j):
        chain = HALVES * layer + h
        blocks = [around(off + 4 * j) for off in theirs + mine]
        wide = jnp.concatenate([x_buf[chain, block] for block in blocks], 0).astype(F32)
        total = jnp.sum(wide * wide, axis=-1, keepdims=True)
        total = jnp.broadcast_to(total, (4 * rows, LANES)).reshape(4, groups, 8, LANES)
        packed = total[:, 0]
        for g in range(1, groups):
            packed = jnp.where(lane8 // span == g, total[:, g], packed)
        scaled = (wide * gain_ref[pl.ds(layer, 1), :]).astype(BF16)
        for p in range(3):
            out = dot(scaled, w_v[layer, :, 2 * width * p : 2 * width * (p + 1)])
            for k in range(2):
                i = 2 * p + k
                piece = out[:, k * width : (k + 1) * width].reshape(4, rows, width)
                for q in range(2):
                    pair_out[chain, blocks[q] // 2, i * rows : (i + 1) * rows] = piece[q].astype(BF16)
                    own_part[h, blocks[2 + q] // 2, i * rows : (i + 1) * rows] = piece[2 + q]
        for q in range(2):
            pair_out[chain, blocks[q] // 2, 6 * rows :] = pair_rows(packed[q]).astype(BF16)
            own_part[h, blocks[2 + q] // 2, 6 * rows : 6 * rows + 8] = packed[2 + q]
        for q in range(2):
            pair_copy(chain, blocks[q] // 2).start()

    def both(chain, h, place):
        arrived = pair_in[chain, place].astype(F32)
        main = own_part[h, place, : 6 * rows] + arrived[: 6 * rows]
        squares = own_part[h, place, 6 * rows : 6 * rows + 8] + (
            arrived[6 * rows : 6 * rows + 8] + arrived[6 * rows + 8 :]
        )
        return main, squares

    def finish(layer, h, j):
        chain = HALVES * layer + h
        for off in mine:
            place = around(off + 4 * j) // 2
            pair_copy(chain, place).wait_recv()
            main, squares = both(chain, h, place)

            @pl.when(place != x)
            def _():
                rs_out[chain, place, : 6 * rows] = main.astype(BF16)
                rs_out[chain, place, 6 * rows :] = pair_rows(squares).astype(BF16)
                rs_copy(chain, place, x).start()

            @pl.when(place == x)
            def _():
                own_part[h, x, : 6 * rows] = main
                own_part[h, x, 6 * rows : 6 * rows + 8] = squares

    def sum_and_advance(layer, h):
        chain = HALVES * layer + h

        def add_sums(off):
            src = lax.rem(x + off, n_x)
            rs_copy(chain, x, src).wait_recv()
            arrived = rs_in[chain, src].astype(F32)
            own_part[h, x, : 6 * rows] += arrived[: 6 * rows]
            own_part[h, x, 6 * rows : 6 * rows + 8] += arrived[6 * rows : 6 * rows + 8] + arrived[6 * rows + 8 :]

        by_distance(n_x, add_sums)

        squares = own_part[h, x, 6 * rows : 6 * rows + 8]
        inv = lax.rsqrt(squares / model + norm_epsilon)
        inv_rows = jnp.concatenate(
            [jnp.broadcast_to(inv[:, span * g : span * g + 1], (8, LANES)) for g in range(groups)], 0
        )
        recept, keys, values, decay_pre, rate_pre, gate_pre = [
            (inv_rows * own_part[h, x, i * rows : (i + 1) * rows]).astype(BF16).astype(F32) for i in range(6)
        ]
        raw = base_ref[pl.ds(layer, 1), :] + decay_pre
        decays = jnp.exp(-jnp.exp(jnp.float32(-0.5)) / (1.0 + jnp.exp(-raw)))
        rates = 1.0 / (1.0 + jnp.exp(-rate_pre))
        unit = keys * lax.rsqrt(dot_split(keys * keys, same_half) + unit_epsilon)
        zero = jnp.zeros_like(keys)
        decays = jnp.where(live_rows[h], decays, 1.0)
        drop = jnp.where(live_rows[h], unit * rates, zero)
        put = jnp.where(live_rows[h], keys, zero)

        def tile_maker(q):
            turned = pltpu.roll(q, HEAD, 1)

            def tiles(n):
                made = []
                for s in range(seqs):
                    at = NEW * s + n
                    made.append(
                        jnp.where(
                            m8,
                            jnp.broadcast_to(q[at : at + 1], (8, LANES)),
                            jnp.broadcast_to(turned[at : at + 1], (8, LANES)),
                        )
                    )
                return jnp.stack(made)[:, None]

            return tiles

        decay_tiles, unit_tiles, drop_tiles, put_tiles, recept_tiles = [
            tile_maker(q) for q in (decays, unit, drop, put, recept)
        ]
        full = (seqs, 8, 8, LANES)
        flat = (seqs * HEAD, LANES)
        memory = st_v[layer, pl.ds(h * seqs * HEAD, seqs * HEAD)].reshape(full)
        reads = jnp.zeros((rows, LANES), F32)
        for n in range(NEW):
            value_rows = jnp.stack(
                [jnp.broadcast_to(values[NEW * s + n : NEW * s + n + 1], (8, LANES)) for s in range(seqs)]
            )[:, None]
            value_full = dot((value_rows * entry).reshape(flat).astype(BF16), spread).reshape(full)
            removed = dot_split((memory * unit_tiles(n)).reshape(flat), same_half).reshape(full)
            memory = memory * decay_tiles(n) - removed * drop_tiles(n) + value_full * put_tiles(n)
            seen = dot_split((memory * recept_tiles(n)).reshape(flat), collect).reshape(full)
            seen = jnp.sum(seen * entry, axis=1).reshape(seqs * 8, LANES)
            pick_shape = (rows, seqs * 8)
            pick = (iota(pick_shape, 0) == (iota(pick_shape, 1) // 8) * NEW + n).astype(F32).astype(BF16)
            seen_high = seen.astype(BF16)
            seen_low = (seen - seen_high.astype(F32)).astype(BF16)
            reads = reads + dot(pick, seen_high) + dot(pick, seen_low)
        states_out[layer, pl.ds(h * seqs * HEAD, seqs * HEAD)] = memory.reshape(flat)

        mean = dot_split(reads, same_half) / HEAD
        dev = reads - mean
        var = dot_split(dev * dev, same_half) / HEAD
        normed = dev * lax.rsqrt(var + group_epsilon) * group_ref[pl.ds(layer, 1), :]
        mixed = jnp.where(live_rows[h], normed / (1.0 + jnp.exp(-gate_pre)), zero)
        mix_buf[chain, d] = mixed.astype(BF16)

        def send_mixed(off):
            d_copy(chain, lax.rem(d + off, n_dp), d).start()

        by_distance(n_dp, send_mixed)

    def project_out(layer, h):
        chain = HALVES * layer + h
        for j in far_first:
            blocks = [around(off + 4 * j) for off in targets + (0,)]
            for block in blocks:
                @pl.when(block != d)
                def _():
                    d_copy(chain, d, block).wait_recv()

            partial = dot(jnp.concatenate([mix_buf[chain, block] for block in blocks], 0), wo_v[layer])
            partial = partial.reshape(4, rows, feats)
            for i, off in enumerate(targets):
                part_out[chain, blocks[i]] = partial[i].astype(BF16)
                near_copy(chain, j, i, blocks[i], around(off)).start()
            class_sum[h, j] = partial[3]

    def sum_classes(layer, h):
        chain = HALVES * layer + h
        for j in far_first:
            total = class_sum[h, j]
            for i in range(3):
                near_copy(chain, j, i, t, t).wait_recv()
                total = total + part_in[chain, 3 * j + i].astype(F32)
            if j:
                far_out[chain, j] = total.astype(BF16)
                far_copy(chain, j, around(4 * j)).start()
            else:
                own_rows[h] = own_rows[h] + total

    def end_block(layer, h):
        chain = HALVES * layer + h
        for j in near_first[1:]:
            far_copy(chain, j, t).wait_recv()
            own_rows[h] = own_rows[h] + far_in[chain, j].astype(F32)
        done = own_rows[h].astype(BF16)
        if layer == 0:
            x_buf[HALVES + h, t] = done
            gather_start(HALVES + h, x_buf.at[HALVES + h, t])
            own_rows[h] = done.astype(F32)
        else:
            tokens_out[pl.ds(h * rows, rows)] = done

    middle, last = near_first[1:-1], near_first[1:][-1:]
    halves = range(HALVES)
    for layer in range(2):
        chains = [HALVES * layer + h for h in halves]
        for h in halves:
            gather_near(chains[h], 0)
            wave(layer, h, 0)
            for j in middle:
                gather_forward(chains[h], j)
        for h in halves:
            finish(layer, h, 0)
        for j in last:
            for h in halves:
                gather_forward(chains[h], j)
        for h in halves:
            for j in middle:
                gather_near(chains[h], j)
                wave(layer, h, j)
        for h in halves:
            for j in middle:
                finish(layer, h, j)
        for j in last:
            for h in halves:
                gather_near(chains[h], j)
                wave(layer, h, j)
            for h in halves:
                finish(layer, h, j)
        for stage in (sum_and_advance, project_out, sum_classes, end_block):
            for h in halves:
                stage(layer, h)

    for chain in range(2 * HALVES):
        for k in range(n_tp - 1):
            g_copy(chain, tokens_ref.at[0], t, t, k).wait_send()
        for j in range(hops):
            for i in range(3):
                near_copy(chain, j, i, t, t).wait_send()
            if j:
                far_copy(chain, j, t).wait_send()

        def drain_d(off):
            d_copy(chain, lax.rem(d + off, n_dp), d).wait_send()

        def drain_rs(off):
            place = lax.rem(x + off, n_x)
            rs_copy(chain, place, x).wait_send()
            pair_copy(chain, place).wait_send()

        by_distance(n_dp, drain_d)
        by_distance(n_x, drain_rs)
        pair_copy(chain, x).wait_send()


def per_device(n_tp, n_dp, tokens, lengths, norm_gain, w_recept, w_keys, w_values, w_decay, w_rate, w_gate,
               decay_base, group_gain, w_out, states):
    rows, feats = tokens.shape
    layers, seqs, heads, flat = states.shape
    folded = flat // LANES
    width = w_recept.shape[2]
    n_x = n_dp // 2
    state_rows = seqs * folded * heads
    packed = states.reshape(layers, seqs, heads, folded, LANES).transpose(0, 1, 3, 2, 4)
    packed = packed.reshape(layers, state_rows, LANES)
    vmem = pl.BlockSpec(memory_space=pltpu.VMEM)
    hbm = pl.BlockSpec(memory_space=pltpu.HBM)
    part = rows // HALVES
    chains = layers * HALVES
    msg = 6 * part + 16
    out, new_states = pl.pallas_call(
        functools.partial(kernel, n_tp, n_dp),
        out_shape=(
            jax.ShapeDtypeStruct((rows, feats), BF16),
            jax.ShapeDtypeStruct((layers, state_rows, LANES), F32),
        ),
        in_specs=[hbm] * 13,
        out_specs=(vmem, vmem),
        scratch_shapes=[
            pltpu.VMEM((HALVES, part, feats), BF16),
            pltpu.SMEM((seqs,), jnp.int32),
            pltpu.VMEM((layers, feats), F32),
            pltpu.VMEM((layers, width), F32),
            pltpu.VMEM((layers, width), F32),
            pltpu.VMEM((layers, feats, 6 * width), BF16),
            pltpu.VMEM((layers, width, feats), BF16),
            pltpu.VMEM((layers, state_rows, LANES), F32),
            pltpu.VMEM((chains, n_tp, part, feats), BF16),
            pltpu.VMEM((chains, n_x, msg, width), BF16),
            pltpu.VMEM((chains, n_x, msg, width), BF16),
            pltpu.VMEM((HALVES, n_x, msg, width), F32),
            pltpu.VMEM((chains, n_x, msg, width), BF16),
            pltpu.VMEM((chains, n_x, msg, width), BF16),
            pltpu.VMEM((chains, n_dp, part, width), BF16),
            pltpu.VMEM((chains, n_tp, part, feats), BF16),
            pltpu.VMEM((chains, 3 * n_tp // 4, part, feats), BF16),
            pltpu.VMEM((HALVES, n_tp // 4, part, feats), F32),
            pltpu.VMEM((chains, n_tp // 4, part, feats), BF16),
            pltpu.VMEM((chains, n_tp // 4, part, feats), BF16),
            pltpu.SemaphoreType.DMA((14,)),
        ] + [pltpu.SemaphoreType.DMA((chains, n_tp))] * 4
        + [pltpu.SemaphoreType.DMA((chains, n_dp))] * 2
        + [pltpu.SemaphoreType.DMA((chains, n_x))] * 4,
        compiler_params=pltpu.CompilerParams(
            collective_id=0, has_side_effects=True, vmem_limit_bytes=48 * 1024 * 1024
        ),
    )(*[
        pltpu.with_memory_space_constraint(operand, pltpu.HBM)
        for operand in (tokens, lengths, norm_gain, decay_base, group_gain,
                        w_recept, w_keys, w_values, w_decay, w_rate, w_gate, w_out, packed)
    ])
    new_states = new_states.reshape(layers, seqs, folded, heads, LANES).transpose(0, 1, 3, 2, 4)
    return out, new_states.reshape(layers, seqs, heads, flat)


def solution(mesh):
    placed = (
        P(("grp", "tp"), "dp"),
        P(("grp", "dp")),
        P(None, "dp"),
        P(None, "dp", "tp"),
        P(None, "dp", "tp"),
        P(None, "dp", "tp"),
        P(None, "dp", "tp"),
        P(None, "dp", "tp"),
        P(None, "dp", "tp"),
        P(None, "tp"),
        P(None, "tp"),
        P(None, "tp", "dp"),
        P(None, ("grp", "dp"), "tp", None),
    )
    return jax.shard_map(
        functools.partial(per_device, mesh.shape["tp"], mesh.shape["dp"]),
        mesh=mesh,
        in_specs=placed,
        out_specs=(P(("grp", "tp"), "dp"), P(None, ("grp", "dp"), "tp", None)),
        check_vma=False,
    )
```

time: 139 us -> 141 us (1.014)
  Pallas kernels: 133 us -> 137 us
  local copies, waits for them, and re-layouts: 3.21 us -> 1.4 us
    pallas_call x1, Pallas kernels: 133 us -> 137 us  [per_device(): pl.pallas_call(functools.partial(kernel, n_tp, n_dp), out_shape=(jax.Shap...]
    unnamed x2, local copies, waits for them, and re-layouts: 3.21 us -> 1.4 us
where the time goes in v3:
time: 141 us; the launch traced here: 139 us
  Pallas kernels  137 us (97%)
    pallas_call x1, Pallas kernels, per_device(): pl.pallas_call(functools.partial(kernel, n_tp, n_dp), out_shape=(jax.Shap...  137 us

profile of v3, /device:TPU:81, one launch (start us, length us, event | category | flops | bytes accessed | tf_op | source)
XLA Modules:
  0.0 138.8 jit_solution(13699461651744159646)
XLA Ops:
  0.6 136.7 %shard_map.140 = (bf16[32,256]{1,0:T(8,128)(2,1)S(1)}, f32[2,512,128]{2,1,0:T(8,128)S(1)}) custom-call(bf16[32,256]{1,0:T(8,128)(2,1)} %tokens_hbm.1, s32[8]{0:T(128)} %lengths_hbm.1, f32[2,256]{1,0:T(2,128)} %gain_hbm.1, f32[2,128]{1,0:T(2,128)} %base_hbm.1, f32[2,128]{1,0:T(2,128)} %group_hbm.1, bf16[2,256,128]{2,1,0:T(8,128)(2,1)} %w0.1, ...), custom_call_target="tpu_custom_call" | custom-call | tf_op jit(solution)/shard_map/pallas_call | solution.py:458
  137.4 0.6 copy.19
  138.0 0.8 copy.20

commit v4 on v3

--- a/solution.py
+++ b/solution.py
@@ -10,7 +10,7 @@
 HEAD = 64
 NEW = 4
 LANES = 128
-HALVES = 2
+HALVES = 1
 norm_epsilon = 1e-06
 unit_epsilon = 0.00064
 group_epsilon = 0.00064

time: 141 us -> 137 us (0.972)
  Pallas kernels: 137 us -> 133 us
    pallas_call x1, Pallas kernels: 137 us -> 133 us  [per_device(): pl.pallas_call(functools.partial(kernel, n_tp, n_dp), out_shape=(jax.Shap...]
where the time goes in v4:
time: 137 us; the launch traced here: 135 us
  Pallas kernels  133 us (97%)
  local copies, waits for them, and re-layouts  1.4 us (1%)
    pallas_call x1, Pallas kernels, per_device(): pl.pallas_call(functools.partial(kernel, n_tp, n_dp), out_shape=(jax.Shap...  133 us

profile of v4, /device:TPU:81, one launch (start us, length us, event | category | flops | bytes accessed | tf_op | source)
XLA Modules:
  0.0 135.0 jit_solution(10174079456785769126)
XLA Ops:
  0.6 132.9 %shard_map.140 = (bf16[32,256]{1,0:T(8,128)(2,1)S(1)}, f32[2,512,128]{2,1,0:T(8,128)S(1)}) custom-call(bf16[32,256]{1,0:T(8,128)(2,1)} %tokens_hbm.1, s32[8]{0:T(128)} %lengths_hbm.1, f32[2,256]{1,0:T(2,128)} %gain_hbm.1, f32[2,128]{1,0:T(2,128)} %base_hbm.1, f32[2,128]{1,0:T(2,128)} %group_hbm.1, bf16[2,256,128]{2,1,0:T(8,128)(2,1)} %w0.1, ...), custom_call_target="tpu_custom_call" | custom-call | tf_op jit(solution)/shard_map/pallas_call | solution.py:458
  133.6 0.6 copy.19
  134.2 0.8 copy.20
